TPU v7x, 32 devices: a whole 2x2x4 slice. The times are simulated.
32 devices in a mesh: sp: 8 (over z, x), dp: 4 (over y, core).
Axes of the slice: x: 2, y: 2, z: 4, core: 2. Of those that a mesh axis runs over, the one named last changes fastest.
Arguments:
- activations: bfloat16 [4, 4096, 2048], P('dp', 'sp'), may hold values from -6 to 6
- value_weight: bfloat16 [2048, 1024], P(('sp', 'dp')), may hold values from -0.125 to 0.125
- gate_weight: bfloat16 [2048, 1024], P(('sp', 'dp')), may hold values from -0.125 to 0.125
- input_weight: bfloat16 [2048, 512], P(('sp', 'dp')), may hold values from -0.125 to 0.125
- readout_weight: bfloat16 [2048, 512], P(('sp', 'dp')), may hold values from -0.125 to 0.125
- rate_weight: bfloat16 [2048, 16], replicated, may hold values from -0.125 to 0.125
- value_taps: bfloat16 [4, 1024], replicated, may hold values from -0.375 to 0.375
- input_taps: bfloat16 [4, 512], replicated, may hold values from -3 to 3
- readout_taps: bfloat16 [4, 512], replicated, may hold values from -3 to 3
- rate_bias: float32 [16], replicated, may hold values from -1 to 1
- decay_log: float32 [16], replicated, may hold values from -1 to 1.5
- norm_gain: float32 [1024], replicated, may hold values from 0.1 to 1.9
- out_weight: bfloat16 [1024, 2048], P(None, ('sp', 'dp')), may hold values from -0.1875 to 0.1875
Outputs:
- mixed_out: bfloat16 [4, 4096, 2048], P('dp', 'sp')
All inputs are finite; a program needn't handle non-finite values.
Results may differ from a plain program's by a relative error of at most 0.014.
Values may be sent and summed in bfloat16 or wider, within the bound.
A program may use at most 128 MiB of HBM per device.

v0:
```python
import jax
import jax.numpy as jnp
from jax import lax
from jax.sharding import PartitionSpec as P

HEADS = 16
HEAD_DIM = 64
GROUPS = 4
STATE = 128
BLOCK = 128


norm_eps = 1.0


def project(rows, weight):
    return jnp.dot(rows, weight, preferred_element_type=jnp.float32).astype(jnp.bfloat16)


def halo_conv(series, kernel, length):
    extent = kernel.shape[0]
    lead = series.shape[0] - length
    padded = series.astype(jnp.float32)
    taps = kernel.astype(jnp.float32)
    result = jnp.zeros((length, series.shape[1]), jnp.float32)
    for offset in range(extent):
        first = lead - extent + 1 + offset
        result = result + taps[offset] * padded[first : first + length]
    return jax.nn.silu(result).astype(jnp.bfloat16)


def exact(equation, left, right):
    return jnp.einsum(equation, left, right, precision=lax.Precision.HIGHEST)


def local_mix(values, inputs, reads, rates, decay):
    length = values.shape[0]
    blocks = length // BLOCK
    share = HEADS // GROUPS
    block_values = values.reshape(blocks, BLOCK, GROUPS, share, HEAD_DIM)
    block_inputs = inputs.reshape(blocks, BLOCK, GROUPS, STATE)
    block_reads = reads.reshape(blocks, BLOCK, GROUPS, STATE)
    block_rates = rates.reshape(blocks, BLOCK, HEADS)
    causal = jnp.tril(jnp.ones((BLOCK, BLOCK), dtype=bool))
    running = exact("ts,bsh->bth", causal.astype(jnp.float32), block_rates * decay)
    by_head = jnp.transpose(running, (0, 2, 1))
    rate_head = jnp.transpose(block_rates, (0, 2, 1))
    intervals = by_head[:, :, :, None] - by_head[:, :, None, :]
    fading = jnp.where(causal, jnp.exp(jnp.minimum(intervals, 0.0)), 0.0)
    fading = fading * rate_head[:, :, None, :]
    intersect = jnp.einsum(
        "btgn,bsgn->bgts", block_reads, block_inputs, preferred_element_type=jnp.float32
    )
    fading = fading.reshape(blocks, GROUPS, share, BLOCK, BLOCK)
    scores = (intersect[:, :, None] * fading).astype(jnp.bfloat16)
    within = jnp.einsum(
        "bgkts,bsgkp->btgkp", scores, block_values, preferred_element_type=jnp.float32
    )
    tail_fade = jnp.exp(running[:, -1:, :] - running) * block_rates
    tail_fade = tail_fade.reshape(blocks, BLOCK, GROUPS, share)
    weighted = (block_values.astype(jnp.float32) * tail_fade[..., None]).astype(jnp.bfloat16)
    states = jnp.einsum(
        "bsgkp,bsgn->bgkpn", weighted, block_inputs, preferred_element_type=jnp.float32
    )
    return within, states, running, block_reads


def entering_states(states, running):
    blocks = states.shape[0]
    share = HEADS // GROUPS
    ends = running[:, -1, :]
    totals = jnp.cumsum(ends, axis=0)
    starts = totals - ends
    left = jnp.exp(totals[-1][None] - totals).reshape(blocks, GROUPS, share)
    last = jnp.sum(left[..., None, None] * states, axis=0)
    devices = lax.axis_size("sp")
    mine = lax.axis_index("sp")
    gathered = lax.all_gather(last.astype(jnp.bfloat16), "sp")
    device_ends = lax.all_gather(totals[-1], "sp")
    device_totals = jnp.cumsum(device_ends, axis=0)
    mine_start = device_totals[mine] - device_ends[mine]
    reach = jnp.exp(jnp.minimum(mine_start[None] - device_totals, 0.0))
    reach = jnp.where((jnp.arange(devices) < mine)[:, None], reach, 0.0)
    reach = reach.reshape(devices, GROUPS, share)
    initial = jnp.sum(reach[..., None, None] * gathered.astype(jnp.float32), axis=0)
    current = initial
    entering = []
    for block in range(blocks):
        entering.append(current)
        fade = jnp.exp(ends[block]).reshape(GROUPS, share, 1, 1)
        current = current * fade + states[block]
    return jnp.stack(entering)


def per_device(
    activations,
    value_weight,
    gate_weight,
    input_weight,
    readout_weight,
    rate_weight,
    value_taps,
    input_taps,
    readout_taps,
    rate_bias,
    decay_log,
    norm_gain,
    out_weight,
):
    sequence = activations[0]
    length = sequence.shape[0]
    devices = lax.axis_size("sp")
    halo = lax.ppermute(sequence[-8:], "sp", [(i, i + 1) for i in range(devices - 1)])
    extended = jnp.concatenate([halo, sequence], axis=0)

    def gathered(weight):
        return lax.all_gather(weight, ("sp", "dp"), axis=0, tiled=True)

    value_full = gathered(value_weight)
    input_full = gathered(input_weight)
    readout_full = gathered(readout_weight)
    gate_full = gathered(gate_weight)
    out_full = gathered(out_weight.T)
    rate_raw = project(sequence, rate_weight)
    rates = jax.nn.softplus(rate_raw.astype(jnp.float32) + rate_bias)
    decay = -jnp.exp(decay_log) / (length * devices)
    values = halo_conv(project(extended, value_full), value_taps, length)
    inputs = halo_conv(project(extended, input_full), input_taps, length)
    reads = halo_conv(project(extended, readout_full), readout_taps, length)
    within, states, running, block_reads = local_mix(values, inputs, reads, rates, decay)
    entering = entering_states(states, running).astype(jnp.bfloat16)
    across = jnp.einsum(
        "btgn,bgkpn->btgkp", block_reads, entering, preferred_element_type=jnp.float32
    )
    fade = jnp.exp(running).reshape(across.shape[:4])
    mixed = (within + across * fade[..., None]).reshape(length, HEADS * HEAD_DIM)
    mixed = mixed.astype(jnp.bfloat16)
    gate_proj = project(sequence, gate_full)
    gated = mixed.astype(jnp.float32) * jax.nn.silu(gate_proj.astype(jnp.float32))
    scale = lax.rsqrt(jnp.mean(gated * gated, axis=-1, keepdims=True) + norm_eps)
    normed = (gated * scale * norm_gain).astype(jnp.bfloat16)
    result = lax.dot_general(
        normed, out_full, (((1,), (1,)), ((), ())), preferred_element_type=jnp.float32
    )
    return result.astype(jnp.bfloat16)[None]


def solution(mesh):
    placed = (
        P("dp", "sp", None),
        P(("sp", "dp"), None),
        P(("sp", "dp"), None),
        P(("sp", "dp"), None),
        P(("sp", "dp"), None),
        P(),
        P(),
        P(),
        P(),
        P(),
        P(),
        P(),
        P(None, ("sp", "dp")),
    )
    return jax.shard_map(
        per_device, mesh=mesh, in_specs=placed, out_specs=P("dp", "sp", None), check_vma=False
    )
```

profile of v0, /device:TPU:24, one launch (start us, length us, event | category | flops | bytes accessed | tf_op | source)
XLA Modules:
  0.0 377.0 jit_solution(2992183182662663084)
XLA Ops:
  8.1 0.8 slice_bitcast_fusion
  8.8 3.4 collective-permute-start
  13.0 2.3 compare_select_fusion
  16.1 50.2 %all-gather.13.cloned.1.call-done = bf16[2048,512]{1,0:T(8,128)(2,1)} async-done(((bf16[64,512]{1,0:T(8,128)(2,1)}), bf16[2048,512]{1,0:T(8,128)(2,1)}) %all-gather.13.cloned.1.call-update) | async-done | bytes 2097168 | tf_op jit(solution)/shard_map/all_gather | solution.py:117
  66.3 2.9 fusion.20
  70.0 59.7 %all-gather.9.cloned.1.call-done = bf16[2048,1024]{1,0:T(8,128)(2,1)} async-done(((bf16[64,1024]{1,0:T(8,128)(2,1)}), bf16[2048,1024]{1,0:T(8,128)(2,1)}) %all-gather.9.cloned.1.call-update) | async-done | bytes 4194320 | tf_op jit(solution)/shard_map/all_gather | solution.py:117
  129.6 4.6 %fusion.18 = f32[520,1024]{1,0:T(8,128)S(1)} fusion(bf16[2048,1024]{1,0:T(8,128)(2,1)} %all-gather.9.cloned.1.call-done, bf16[512,2048]{1,0:T(8,128)(2,1)S(1)} %bitcast.97, bf16[8,2048]{1,0:T(8,128)(2,1)S(1)} %collective-permute-done), kind=kOutput, calls=%fused_computation.35 | convolution fusion | flops 2186362880 | bytes 8454144 | tf_op jit(solution)/shard_map/dot_general | solution.py:17
  134.2 1.3 multiply_convert_fusion.4
  137.3 1.2 multiply_reduce_fusion.1
  139.7 15.9 %all-gather.1 = f32[8,1,16]{2,1,0:T(1,128)S(1)} all-gather(f32[1,1,16]{2,1,0:T(1,128)S(1)} %get-tuple-element.25), channel_id=1, replica_groups=mesh['sp'=8,'dp'=4] {'sp'}, dimensions={0}, use_global_device_ids=true | all-gather | bytes 576 | tf_op jit(solution)/shard_map/all_gather | solution.py:79
  156.5 31.1 %all-gather.11.cloned.1.call-done = bf16[2048,512]{1,0:T(8,128)(2,1)} async-done(((bf16[64,512]{1,0:T(8,128)(2,1)}), bf16[2048,512]{1,0:T(8,128)(2,1)}) %all-gather.11.cloned.1.call-update) | async-done | bytes 2097168 | tf_op jit(solution)/shard_map/all_gather | solution.py:117
  187.6 3.5 fusion.21
  191.1 1.5 multiply_convert_fusion.7
  192.6 1.2 reshape.123
  195.0 3.1 fusion.2
  198.1 39.2 %all-gather.19.cloned.1.call-done = bf16[32,4,64,128]{3,2,1,0:T(8,128)(2,1)} async-done(((bf16[4,4,64,128]{3,2,1,0:T(8,128)(2,1)}), bf16[32,4,64,128]{3,2,1,0:T(8,128)(2,1)}) %all-gather.19.cloned.1.call-update) | async-done | bytes 2097168 | tf_op jit(solution)/shard_map/all_gather | solution.py:78
  237.3 2.1 fusion
  239.8 1.2 copy-done.5
  241.5 3.4 copy.58
  244.9 5.8 %reshape.135 = f32[512,1024]{1,0:T(8,128)} reshape(f32[4,128,4,4,64]{4,3,2,1,0:T(4,128)} %copy.58) | data formatting | bytes 4194304 | tf_op jit(solution)/shard_map/convert_element_type | solution.py:139
  250.7 49.8 %all-gather.15.cloned.1.call-done = bf16[2048,1024]{1,0:T(8,128)(2,1)} async-done(((bf16[64,1024]{1,0:T(8,128)(2,1)}), bf16[2048,1024]{1,0:T(8,128)(2,1)}) %all-gather.15.cloned.1.call-update) | async-done | bytes 4194320 | tf_op jit(solution)/shard_map/all_gather | solution.py:117
  300.4 6.9 %multiply_reduce_fusion = (f32[512]{0:T(512)S(1)}, f32[512,1024]{1,0:T(8,128)}) fusion(f32[512,1024]{1,0:T(8,128)} %reshape.135, bf16[2048,1024]{1,0:T(8,128)(2,1)} %all-gather.15.cloned.1.call-done, bf16[1,512,2048]{2,1,0:T(8,128)(2,1)S(1)} %copy-done.4), kind=kOutput, calls=%fused_computation.24 | convolution fusion | flops 2152201728 | bytes 10487808 | tf_op jit(solution)/shard_map/dot_general | solution.py:17
  307.3 56.3 %all-gather.17.cloned.1.call-done = bf16[2048,1024]{1,0:T(8,128)(2,1)} async-done(((bf16[64,1024]{1,0:T(8,128)(2,1)}), bf16[2048,1024]{1,0:T(8,128)(2,1)}) %all-gather.17.cloned.1.call-update) | async-done | bytes 4194320 | tf_op jit(solution)/shard_map/all_gather | solution.py:117
  363.6 6.5 %fusion.1 = bf16[1,512,2048]{2,1,0:T(8,128)(2,1)} fusion(bf16[2048,1024]{1,0:T(8,128)(2,1)} %all-gather.17.cloned.1.call-done, f32[512,1024]{1,0:T(8,128)} %get-tuple-element.30, f32[1024]{0:T(1024)S(1)} %copy-done.9, f32[512]{0:T(512)S(1)} %add_rsqrt_fusion), kind=kOutput, calls=%fused_computation.4 | convolution fusion | flops 2150105088 | bytes 8394752 | tf_op jit(solution)/shard_map/dot_general | solution.py:142
  (71 shorter events, 9.7 us)
Async XLA Ops:
  6.5 6.4 %copy-start = (bf16[2048,16]{0,1:T(8,128)(2,1)S(1)}, bf16[2048,16]{0,1:T(8,128)(2,1)}, u32[]{:S(2)}) copy-start(bf16[2048,16]{0,1:T(8,128)(2,1)} %param.18) | copy-start | bytes 196612
  6.5 59.8 %copy-start.3 = (bf16[1,512,2048]{2,1,0:T(8,128)(2,1)S(1)}, bf16[1,512,2048]{2,1,0:T(8,128)(2,1)}, u32[]{:S(2)}) copy-start(bf16[1,512,2048]{2,1,0:T(8,128)(2,1)} %param.13) | copy-start | bytes 6291460
  6.5 9.4 %copy-start.6 = (bf16[4,1024]{1,0:T(4,128)(2,1)S(1)}, bf16[4,1024]{1,0:T(4,128)(2,1)}, u32[]{:S(2)}) copy-start(bf16[4,1024]{1,0:T(4,128)(2,1)} %param.19) | copy-start | bytes 24580
  6.5 9.5 %copy-start.7 = (bf16[4,512]{1,0:T(4,128)(2,1)S(1)}, bf16[4,512]{1,0:T(4,128)(2,1)}, u32[]{:S(2)}) copy-start(bf16[4,512]{1,0:T(4,128)(2,1)} %param.20) | copy-start | bytes 12292
  6.5 59.8 %all-gather.13.cloned.1.call-start = ((), (), s32[]{:S(2)}) async-start(), calls=%async_computation.2 | async-start | bytes 2162688 | tf_op jit(solution)/shard_map/all_gather | solution.py:117
  7.3 122.3 %all-gather.9.cloned.1.call-start = ((), (), s32[]{:S(2)}) async-start(), calls=%async_computation | async-start | bytes 4325376 | tf_op jit(solution)/shard_map/all_gather | solution.py:117
  8.0 179.6 %all-gather.11.cloned.1.call-start = ((), (), s32[]{:S(2)}) async-start(), calls=%async_computation.1 | async-start | bytes 2162688 | tf_op jit(solution)/shard_map/all_gather | solution.py:117
  8.8 7.2 %collective-permute-start = (bf16[8,2048]{1,0:T(8,128)(2,1)S(1)}, bf16[8,2048]{1,0:T(8,128)(2,1)S(1)}, u32[]{:S(2)}, u32[]{:S(2)}) collective-permute-start(bf16[8,2048]{1,0:T(8,128)(2,1)S(1)} %slice_bitcast_fusion), channel_id=1, source_target_pairs={{0,4},{4,8},{8,12},{12,16},{16,20},{20,24},{24,28},{1,5},{5,9},{9,... | collective-permute-start | bytes 98312 | tf_op jit(solution)/shard_map/ppermute | solution.py:113
  12.3 225.0 %all-gather.19.cloned.1.call-start = ((), (), s32[]{:S(2)}) async-start(), calls=%async_computation.5 | async-start | bytes 2359296 | tf_op jit(solution)/shard_map/all_gather | solution.py:78
  136.3 1.0 copy-start.1
  137.3 19.2 %copy-start.8 = (bf16[4,512]{1,0:T(4,128)(2,1)S(1)}, bf16[4,512]{1,0:T(4,128)(2,1)}, u32[]{:S(2)}) copy-start(bf16[4,512]{1,0:T(4,128)(2,1)} %param.21) | copy-start | bytes 12292
  138.5 161.9 %all-gather.15.cloned.1.call-start = ((), (), s32[]{:S(2)}) async-start(), calls=%async_computation.3 | async-start | bytes 4325376 | tf_op jit(solution)/shard_map/all_gather | solution.py:117
  139.1 224.5 %all-gather.17.cloned.1.call-start = ((), (), s32[]{:S(2)}) async-start(), calls=%async_computation.4 | async-start | bytes 4325376 | tf_op jit(solution)/shard_map/all_gather | solution.py:117
  193.7 1.2 copy-start.2
  239.4 1.6 copy-start.5
  244.9 55.6 %copy-start.4 = (bf16[1,512,2048]{2,1,0:T(8,128)(2,1)S(1)}, bf16[1,512,2048]{2,1,0:T(8,128)(2,1)}, u32[]{:S(2)}) copy-start(bf16[1,512,2048]{2,1,0:T(8,128)(2,1)} %param.13) | copy-start | bytes 6291460
  250.7 112.9 %copy-start.9 = (f32[1024]{0:T(1024)S(1)}, f32[1024]{0:T(1024)}, u32[]{:S(2)}) copy-start(f32[1024]{0:T(1024)} %param.24) | copy-start | bytes 12292
Sparse Core Ops, SparseCore 0:
  10.2 56.0 all-gather.12
  69.2 60.3 all-gather.8
  132.5 55.0 all-gather.10
  189.6 47.6 all-gather.18
  240.0 60.3 all-gather.14
  303.2 60.3 all-gather.16
where the time goes:
time: 380 us; the launch traced here: 377 us
  waiting for transfers between devices  289 us (76%)
  matrix products  32.1 us (8%)
  blocking collectives  15.9 us (4%)
  local copies, waits for them, and re-layouts  15.6 us (4%)
  between operations  13.7 us (4%)
  other arithmetic  7.33 us (2%)
    all_gather x5, waiting for transfers between devices, gathered(): return lax.all_gather(weight, ('sp', 'dp'), axis=0, tiled=True)  247 us
    all_gather x1, waiting for transfers between devices, entering_states(): gathered = lax.all_gather(last.astype(jnp.bfloat16), 'sp')  39.2 us
    dot_general x5, matrix products, project(): jnp.dot(rows, weight, preferred_element_type=jnp.float32)  20 us
    all_gather x1, blocking collectives, entering_states(): device_ends = lax.all_gather(totals[-1], 'sp')  15.9 us
    convert_element_type x2, local copies, waits for them, and re-layouts, per_device(): mixed.astype(jnp.float32) * jax.nn.silu(gate_proj.astype(jnp.float32))  9.15 us
  transfers between devices with their start and end apart: 7, of which 6 were waited for; matrix products, arithmetic and copies ran while one was open for 12% of the time, Pallas kernels for 0%

commit v1 on v0

--- a/solution.py
+++ b/solution.py
@@ -1,6 +1,11 @@
+import functools
+import itertools
+
 import jax
 import jax.numpy as jnp
 from jax import lax
+from jax.experimental import pallas as pl
+from jax.experimental.pallas import tpu as pltpu
 from jax.sharding import PartitionSpec as P
 
 HEADS = 16
@@ -11,6 +16,159 @@
 
 
 norm_eps = 1.0
+
+
+def nearest(count, place, rank):
+    found = 0
+    for start in range(count):
+        order = sorted(range(count), key=lambda other: (abs(other - start), other))
+        found = found + jnp.where(place == start, order[rank], 0)
+    return found
+
+
+def onward(count, place, origin, rank):
+    if count == 2:
+        return [(1 - place, None)] if rank == 0 else []
+    steps = [1, -1] if rank == 0 else [jnp.where(origin < place, 1, -1)]
+    pairs = []
+    for step in steps:
+        target = place + step
+        pairs.append((target, jnp.logical_and(target >= 0, target < count)))
+    return [pair for pair in pairs if count > 1]
+
+
+def when(exists, action):
+    if exists is None:
+        action()
+    else:
+        pl.when(exists)(action)
+
+
+def gather_kernel(lines, own_ref, full_ref, send_sem, recv_sem, pair_sem, local_sem):
+    depth, across, along, cores = lines
+    sp = lax.axis_index("sp")
+    dp = lax.axis_index("dp")
+    here = (sp // across, sp % across, dp // cores)
+    core = dp % cores
+    counts = (depth, across, along)
+
+    def target_id(place, which):
+        return {"sp": place[0] * across + place[1], "dp": place[2] * cores + which}
+
+    def moved(dim, value):
+        return tuple(value if d == dim else here[d] for d in range(3))
+
+    barrier = pltpu.get_barrier_semaphore()
+    for dim in range(3):
+        for target, exists in onward(counts[dim], here[dim], here[dim], 0):
+
+            def greet(dim=dim, target=target):
+                pl.semaphore_signal(
+                    barrier,
+                    inc=1,
+                    device_id=target_id(moved(dim, target), core),
+                    device_id_type=pl.DeviceIdType.MESH,
+                )
+
+            when(exists, greet)
+    pl.semaphore_signal(
+        barrier,
+        inc=1,
+        device_id=target_id(here, 1 - core),
+        device_id_type=pl.DeviceIdType.MESH,
+    )
+    peers = 1
+    for dim in range(3):
+        for target, exists in onward(counts[dim], here[dim], here[dim], 0):
+            peers = peers + (1 if exists is None else jnp.where(exists, 1, 0))
+    pl.semaphore_wait(barrier, peers)
+
+    def chip_of(place):
+        return (place[0] * across + place[1]) * along + place[2]
+
+    mine = chip_of(here) * cores + core
+    local = pltpu.make_async_copy(own_ref, full_ref.at[mine], local_sem)
+    local.start()
+    ranks = sorted(itertools.product(*(range(n) for n in counts)), key=lambda r: (sum(r), r))
+    used = 0
+    started = []
+    arrivals = []
+    for rank in ranks:
+        origin = tuple(nearest(counts[d], here[d], rank[d]) for d in range(3))
+        chip = chip_of(origin)
+        block = chip * cores + core
+        for half in range(2):
+            landed = full_ref.at[block, half]
+            source = own_ref.at[half] if sum(rank) == 0 else landed
+            if sum(rank):
+                pltpu.make_async_remote_copy(
+                    src_ref=landed,
+                    dst_ref=landed,
+                    send_sem=send_sem.at[0],
+                    recv_sem=recv_sem.at[chip, half],
+                    device_id=target_id(here, 1 - core),
+                    device_id_type=pl.DeviceIdType.MESH,
+                ).wait_recv()
+            order = (0, 1, 2) if half == 0 else (0, 2, 1)
+            hops = []
+            for position in (2, 1, 0):
+                if any(rank[order[later]] for later in range(position + 1, 3)):
+                    continue
+                dim = order[position]
+                for target, exists in onward(counts[dim], here[dim], origin[dim], rank[dim]):
+                    hops.append((target_id(moved(dim, target), core), recv_sem, exists))
+            hops.append((target_id(here, 1 - core), pair_sem, None))
+            for device, sem, exists in hops:
+                copy = pltpu.make_async_remote_copy(
+                    src_ref=source,
+                    dst_ref=landed,
+                    send_sem=send_sem.at[used],
+                    recv_sem=sem.at[chip, half],
+                    device_id=device,
+                    device_id_type=pl.DeviceIdType.MESH,
+                )
+                used += 1
+                when(exists, copy.start)
+                started.append((copy, exists))
+    for copy, exists in started:
+        when(exists, copy.wait_send)
+    for chip in range(depth * across * along):
+        for half in range(2):
+            landed = full_ref.at[chip * cores + 1 - core, half]
+            pltpu.make_async_remote_copy(
+                src_ref=landed,
+                dst_ref=landed,
+                send_sem=send_sem.at[0],
+                recv_sem=pair_sem.at[chip, half],
+                device_id=target_id(here, 1 - core),
+                device_id_type=pl.DeviceIdType.MESH,
+            ).wait_recv()
+    local.wait()
+
+
+def gather_rows(own):
+    sp, dp = lax.axis_size("sp"), lax.axis_size("dp")
+    across = 1
+    while 4 * across * across <= sp:
+        across *= 2
+    lines = (sp // across, across, dp // 2, 2)
+    chips = sp * dp // 2
+    rows, columns = own.shape
+    hops = 2 * chips * 7
+    full = pl.pallas_call(
+        functools.partial(gather_kernel, lines),
+        out_shape=jax.ShapeDtypeStruct((sp * dp, 2, rows // 2, columns), own.dtype),
+        in_specs=[pl.BlockSpec(memory_space=pltpu.VMEM)],
+        out_specs=pl.BlockSpec(memory_space=pl.ANY),
+        scratch_shapes=[
+            pltpu.SemaphoreType.DMA((hops,)),
+            pltpu.SemaphoreType.DMA((chips, 2)),
+            pltpu.SemaphoreType.DMA((chips, 2)),
+            pltpu.SemaphoreType.DMA,
+        ],
+        compiler_params=pltpu.CompilerParams(collective_id=1, has_side_effects=True),
+    )(own.reshape(2, rows // 2, columns))
+    return full.reshape(sp * dp * rows, columns)
 
 
 def project(rows, weight):
@@ -74,15 +232,17 @@
     left = jnp.exp(totals[-1][None] - totals).reshape(blocks, GROUPS, share)
     last = jnp.sum(left[..., None, None] * states, axis=0)
     devices = lax.axis_size("sp")
-    mine = lax.axis_index("sp")
-    gathered = lax.all_gather(last.astype(jnp.bfloat16), "sp")
-    device_ends = lax.all_gather(totals[-1], "sp")
-    device_totals = jnp.cumsum(device_ends, axis=0)
-    mine_start = device_totals[mine] - device_ends[mine]
-    reach = jnp.exp(jnp.minimum(mine_start[None] - device_totals, 0.0))
-    reach = jnp.where((jnp.arange(devices) < mine)[:, None], reach, 0.0)
-    reach = reach.reshape(devices, GROUPS, share)
-    initial = jnp.sum(reach[..., None, None] * gathered.astype(jnp.float32), axis=0)
+    held = last
+    span = totals[-1]
+    stride = 1
+    while stride < devices:
+        pairs = [(i, i + stride) for i in range(devices - stride)]
+        came = lax.ppermute(held.astype(jnp.bfloat16), "sp", pairs).astype(jnp.float32)
+        held = held + jnp.exp(span).reshape(GROUPS, share, 1, 1) * came
+        span = span + lax.ppermute(span, "sp", pairs)
+        stride *= 2
+    pairs = [(i, i + 1) for i in range(devices - 1)]
+    initial = lax.ppermute(held.astype(jnp.bfloat16), "sp", pairs).astype(jnp.float32)
     current = initial
     entering = []
     for block in range(blocks):
@@ -113,20 +273,20 @@
     halo = lax.ppermute(sequence[-8:], "sp", [(i, i + 1) for i in range(devices - 1)])
     extended = jnp.concatenate([halo, sequence], axis=0)
 
-    def gathered(weight):
-        return lax.all_gather(weight, ("sp", "dp"), axis=0, tiled=True)
-
-    value_full = gathered(value_weight)
-    input_full = gathered(input_weight)
-    readout_full = gathered(readout_weight)
-    gate_full = gathered(gate_weight)
-    out_full = gathered(out_weight.T)
+    own = jnp.concatenate(
+        [value_weight, input_weight, readout_weight, gate_weight, out_weight.T], axis=1
+    )
+    full = gather_rows(own)
+    ends = [0]
+    for weight in (value_weight, input_weight, readout_weight, gate_weight):
+        ends.append(ends[-1] + weight.shape[1])
     rate_raw = project(sequence, rate_weight)
     rates = jax.nn.softplus(rate_raw.astype(jnp.float32) + rate_bias)
     decay = -jnp.exp(decay_log) / (length * devices)
-    values = halo_conv(project(extended, value_full), value_taps, length)
-    inputs = halo_conv(project(extended, input_full), input_taps, length)
-    reads = halo_conv(project(extended, readout_full), readout_taps, length)
+    projected = project(extended, full[:, : ends[4]])
+    values = halo_conv(projected[:, ends[0] : ends[1]], value_taps, length)
+    inputs = halo_conv(projected[:, ends[1] : ends[2]], input_taps, length)
+    reads = halo_conv(projected[:, ends[2] : ends[3]], readout_taps, length)
     within, states, running, block_reads = local_mix(values, inputs, reads, rates, decay)
     entering = entering_states(states, running).astype(jnp.bfloat16)
     across = jnp.einsum(
@@ -135,12 +295,12 @@
     fade = jnp.exp(running).reshape(across.shape[:4])
     mixed = (within + across * fade[..., None]).reshape(length, HEADS * HEAD_DIM)
     mixed = mixed.astype(jnp.bfloat16)
-    gate_proj = project(sequence, gate_full)
+    gate_proj = projected[halo.shape[0] :, ends[3] : ends[4]]
     gated = mixed.astype(jnp.float32) * jax.nn.silu(gate_proj.astype(jnp.float32))
     scale = lax.rsqrt(jnp.mean(gated * gated, axis=-1, keepdims=True) + norm_eps)
     normed = (gated * scale * norm_gain).astype(jnp.bfloat16)
     result = lax.dot_general(
-        normed, out_full, (((1,), (1,)), ((), ())), preferred_element_type=jnp.float32
+        normed, full[:, ends[4] :], (((1,), (1,)), ((), ())), preferred_element_type=jnp.float32
     )
     return result.astype(jnp.bfloat16)[None]
 

time: 380 us -> 184 us (0.48)
  waiting for transfers between devices: 289 us -> 34.5 us
  Pallas kernels: 0 us -> 83.8 us
  blocking collectives: 15.9 us -> 0 us
  between operations: 13.7 us -> 0.58 us
  starting transfers between devices: 3.62 us -> 14 us
  matrix products: 32.1 us -> 23.2 us
    all_gather x6 -> x0, waiting for transfers between devices: 286 us -> none  [the longest x5 247 us: gathered(): return lax.all_gather(weight, ('sp', 'dp'), axis=0, tiled=True)]
    pallas_call x0 -> x1, Pallas kernels: none -> 83.8 us  [gather_rows(): pl.pallas_call(functools.partial(gather_kernel, lines), out_shape=jax.Sha...]
    ppermute x0 -> x6, waiting for transfers between devices: none -> 34.5 us  [the longest x4 30.4 us: entering_states(): lax.ppermute(held.astype(jnp.bfloat16), 'sp', pairs).astype(jnp.float32)]
    all_gather x1 -> x0, blocking collectives: 15.9 us -> none  [entering_states(): device_ends = lax.all_gather(totals[-1], 'sp')]
    ppermute x0 -> x6, starting transfers between devices: none -> 10.7 us  [the longest x4 7.44 us: entering_states(): lax.ppermute(held.astype(jnp.bfloat16), 'sp', pairs).astype(jnp.float32)]
    dot_general x5 -> x2, matrix products: 20 us -> 12 us  [project(): jnp.dot(rows, weight, preferred_element_type=jnp.float32)]
  transfers between devices with their start and end apart: 7 -> 7, of which waited for: 6 -> 5; matrix products, arithmetic and copies ran while one was open for 12% -> 17% of each run, Pallas kernels for 0% -> 46%
where the time goes in v1:
time: 184 us
  Pallas kernels  83.8 us (46%)
  waiting for transfers between devices  34.5 us (19%)
  matrix products  23.2 us (13%)
  local copies, waits for them, and re-layouts  18 us (10%)
  starting transfers between devices  14 us (8%)
  other arithmetic  9.32 us (5%)
    pallas_call x1, Pallas kernels, gather_rows(): pl.pallas_call(functools.partial(gather_kernel, lines), out_shape=jax.Sha...  83.8 us
    ppermute x4, waiting for transfers between devices, entering_states(): lax.ppermute(held.astype(jnp.bfloat16), 'sp', pairs).astype(jnp.float32)  30.4 us
    dot_general x2, matrix products, project(): jnp.dot(rows, weight, preferred_element_type=jnp.float32)  12 us
    convert_element_type x2, local copies, waits for them, and re-layouts, per_device(): mixed.astype(jnp.float32) * jax.nn.silu(gate_proj.astype(jnp.float32))  7.86 us
    ppermute x4, starting transfers between devices, entering_states(): lax.ppermute(held.astype(jnp.bfloat16), 'sp', pairs).astype(jnp.float32)  7.44 us
    dot_general x1, matrix products, per_device(): lax.dot_general(normed, full[:, ends[4]:], (((1,), (1,)), ((), ())), pref...  6.64 us
    ppermute x2, waiting for transfers between devices, entering_states(): span = span + lax.ppermute(span, 'sp', pairs)  4.08 us
  transfers between devices with their start and end apart: 7, of which 5 were waited for; matrix products, arithmetic and copies ran while one was open for 17% of the time, Pallas kernels for 46%

profile of v1, /device:TPU:24, one launch (start us, length us, event | category | flops | bytes accessed | tf_op | source)
XLA Modules:
  0.0 183.5 jit_solution(14752303923317266853)
XLA Ops:
  1.0 3.4 %collective-permute-start = (bf16[8,2048]{1,0:T(8,128)(2,1)S(1)}, bf16[8,2048]{1,0:T(8,128)(2,1)S(1)}, u32[]{:S(2)}, u32[]{:S(2)}) collective-permute-start(bf16[8,2048]{1,0:T(8,128)(2,1)S(1)} %slice_bitcast_fusion.3), channel_id=1, source_target_pairs={{0,4},{4,8},{8,12},{12,16},{16,20},{20,24},{24,28},{1,5},{5,9},{9,... | collective-permute-start | bytes 98312 | tf_op jit(solution)/shard_map/ppermute | solution.py:273
  5.0 2.3 %compare_select_fusion = f32[512,16]{0,1:T(8,128)S(1)} fusion(bf16[2048,16]{0,1:T(8,128)(2,1)S(1)} %copy-done, f32[16]{0:T(128)} %param.22, bf16[1,512,2048]{2,1,0:T(8,128)(2,1)} %param.13), kind=kOutput, calls=%fused_computation.97 | convolution fusion | flops 33628160 | bytes 2195520 | tf_op jit(solution)/shard_map/dot_general | solution.py:175
  7.8 1.9 %collective-permute-start.2 = (f32[16]{0:T(128)S(1)}, f32[16]{0:T(128)S(1)}, u32[]{:S(2)}, u32[]{:S(2)}) collective-permute-start(f32[16]{0:T(128)S(1)} %get-tuple-element.29), channel_id=1, source_target_pairs={{0,4},{4,8},{8,12},{12,16},{16,20},{20,24},{24,28},{1,5},{5,9},{9,... | collective-permute-start | bytes 200 | tf_op jit(solution)/shard_map/ppermute | solution.py:242
  12.3 83.8 %shard_map.127 = bf16[32,2,32,4096]{3,2,1,0:T(8,128)(2,1)} custom-call(bf16[2,32,4096]{2,1,0:T(8,128)(2,1)} %bitcast.118), custom_call_target="tpu_custom_call" | custom-call | tf_op jit(solution)/shard_map/pallas_call | solution.py:158
  98.8 9.7 %fusion.2 = bf16[520,3072]{1,0:T(8,128)(2,1)S(1)} fusion(bf16[2048,4096]{1,0:T(8,128)(2,1)} %bitcast.113, bf16[512,2048]{1,0:T(8,128)(2,1)S(1)} %bitcast.116, bf16[8,2048]{1,0:T(8,128)(2,1)S(1)} %collective-permute-done), kind=kOutput, calls=%fused_computation.2 | convolution fusion | flops 6548971520 | bytes 17907712 | tf_op jit(solution)/shard_map/dot_general | solution.py:175
  111.5 1.3 copy.22
  112.8 1.3 reshape.99
  114.2 1.4 multiply_convert_fusion.6
  117.3 1.8 %multiply_reduce_fusion.1 = (f32[4,4,64,128]{3,2,1,0:T(8,128)S(1)}, f32[4,4,4,64,128]{4,3,2,1,0:T(8,128)}) fusion(f32[4,4,4]{2,1,0:T(4,128)S(1)} %bitcast.125, bf16[4,128,4,128,1]{3,2,1,0,4:T(4,128)(2,1)S(1)} %bitcast.115, bf16[4,128,4,4,64]{1,0,4,3,2:T(4,128)(2,1)S(1)} %multiply_convert_fusion.3), kind=kOutput, calls=%fused_computation.30 | convolution fusion | flops 135135232 | bytes 4194560 | tf_op jit(solution)/shard_map/bsgkp,bsgn->bgkpn/dot_general | solution.py:220
  119.2 1.9 %collective-permute-start.1 = (bf16[4,4,64,128]{3,2,1,0:T(8,128)(2,1)S(1)}, bf16[4,4,64,128]{3,2,1,0:T(8,128)(2,1)S(1)}, u32[]{:S(2)}, u32[]{:S(2)}) collective-permute-start(bf16[4,4,64,128]{3,2,1,0:T(8,128)(2,1)S(1)} %convert_element_type.105), channel_id=1, source_target_pairs={{0,4},{4,8},{8,12},{12,16},{16,20},{20,24},{24,28},{1,5},{5,9},{9,... | collective-permute-start | bytes 786440 | tf_op jit(solution)/shard_map/ppermute | solution.py:240
  121.2 1.3 collective-permute-start.4
  122.5 4.1 %collective-permute-done.4 = f32[16]{0:T(128)S(1)} collective-permute-done((f32[16]{0:T(128)S(1)}, f32[16]{0:T(128)S(1)}, u32[]{:S(2)}, u32[]{:S(2)}) %collective-permute-start.4) | collective-permute-done | bytes 96 | tf_op jit(solution)/shard_map/ppermute | solution.py:242
  126.7 3.9 %collective-permute-done.1 = bf16[4,4,64,128]{3,2,1,0:T(8,128)(2,1)S(1)} collective-permute-done((bf16[4,4,64,128]{3,2,1,0:T(8,128)(2,1)S(1)}, bf16[4,4,64,128]{3,2,1,0:T(8,128)(2,1)S(1)}, u32[]{:S(2)}, u32[]{:S(2)}) %collective-permute-start.1) | collective-permute-done | bytes 262176 | tf_op jit(solution)/shard_map/ppermute | solution.py:240
  130.7 1.3 collective-permute-start.3
  132.8 7.5 %collective-permute-done.3 = bf16[4,4,64,128]{3,2,1,0:T(8,128)(2,1)S(1)} collective-permute-done((bf16[4,4,64,128]{3,2,1,0:T(8,128)(2,1)S(1)}, bf16[4,4,64,128]{3,2,1,0:T(8,128)(2,1)S(1)}, u32[]{:S(2)}, u32[]{:S(2)}) %collective-permute-start.3) | collective-permute-done | bytes 262176 | tf_op jit(solution)/shard_map/ppermute | solution.py:240
  140.5 1.4 collective-permute-start.5
  142.5 12.5 %collective-permute-done.5 = bf16[4,4,64,128]{3,2,1,0:T(8,128)(2,1)S(1)} collective-permute-done((bf16[4,4,64,128]{3,2,1,0:T(8,128)(2,1)S(1)}, bf16[4,4,64,128]{3,2,1,0:T(8,128)(2,1)S(1)}, u32[]{:S(2)}, u32[]{:S(2)}) %collective-permute-start.5) | collective-permute-done | bytes 262176 | tf_op jit(solution)/shard_map/ppermute | solution.py:240
  155.2 2.8 %collective-permute-start.6 = (bf16[4,4,64,128]{3,2,1,0:T(8,128)(2,1)S(1)}, bf16[4,4,64,128]{3,2,1,0:T(8,128)(2,1)S(1)}, u32[]{:S(2)}, u32[]{:S(2)}) collective-permute-start(bf16[4,4,64,128]{3,2,1,0:T(8,128)(2,1)S(1)} %add_convert_fusion), channel_id=1, source_target_pairs={{0,4},{4,8},{8,12},{12,16},{16,20},{20,24},{24,28},{1,5},{5,9},{9,... | collective-permute-start | bytes 786440 | tf_op jit(solution)/shard_map/ppermute | solution.py:245
  158.1 1.6 fusion.16
  159.7 6.6 %collective-permute-done.6 = bf16[4,4,64,128]{3,2,1,0:T(8,128)(2,1)S(1)} collective-permute-done((bf16[4,4,64,128]{3,2,1,0:T(8,128)(2,1)S(1)}, bf16[4,4,64,128]{3,2,1,0:T(8,128)(2,1)S(1)}, u32[]{:S(2)}, u32[]{:S(2)}) %collective-permute-start.6) | collective-permute-done | bytes 262176 | tf_op jit(solution)/shard_map/ppermute | solution.py:245
  167.1 3.3 %copy.38 = f32[4,128,4,4,64]{4,3,2,1,0:T(4,128)} copy(f32[4,128,4,4,64]{1,4,3,2,0:T(8,128)S(1)} %fusion.32) | data formatting | bytes 4194304 | tf_op jit(solution)/shard_map/convert_element_type | solution.py:299
  170.4 4.5 %reshape.107 = f32[512,1024]{1,0:T(8,128)S(1)} reshape(f32[4,128,4,4,64]{4,3,2,1,0:T(4,128)} %copy.38) | data formatting | bytes 4194304 | tf_op jit(solution)/shard_map/convert_element_type | solution.py:299
  174.9 1.9 %multiply_reduce_fusion = f32[512]{0:T(512)S(1)} fusion(f32[512,1024]{1,0:T(8,128)S(1)} %reshape.107, bf16[520,3072]{1,0:T(8,128)(2,1)} %copy-done.4), kind=kLoop, calls=%fused_computation.29 | loop fusion | flops 4193792 | bytes 3147776 | tf_op jit(solution)/shard_map/reduce_sum | solution.py:300
  176.9 6.6 %fusion.10 = bf16[1,512,2048]{2,1,0:T(8,128)(2,1)} fusion(bf16[2048,4096]{1,0:T(8,128)(2,1)} %bitcast.114, f32[1024]{0:T(1024)S(1)} %copy-done.22, f32[512]{0:T(512)S(1)} %add_rsqrt_fusion, f32[512,1024]{1,0:T(8,128)S(1)} %reshape.107, bf16[520,3072]{1,0:T(8,128)(2,1)} %copy-done.4), kind=kOutput, calls=%fused_computation.7 | convolution fusion | flops 2153250816 | bytes 9443328 | tf_op jit(solution)/shard_map/dot_general | solution.py:302
  (95 shorter events, 14.6 us)
Async XLA Ops:
  0.0 10.6 %copy-start.8 = (bf16[64,1024]{1,0:T(8,128)(2,1)S(1)}, bf16[64,1024]{1,0:T(8,128)(2,1)}, u32[]{:S(2)}) copy-start(bf16[64,1024]{1,0:T(8,128)(2,1)} %param.14) | copy-start | bytes 393220
  0.0 10.6 %copy-start.14 = (bf16[4,1024]{1,0:T(4,128)(2,1)S(1)}, bf16[4,1024]{1,0:T(4,128)(2,1)}, u32[]{:S(2)}) copy-start(bf16[4,1024]{1,0:T(4,128)(2,1)} %param.19) | copy-start | bytes 24580
  0.0 10.7 %copy-start.16 = (bf16[4,512]{1,0:T(4,128)(2,1)S(1)}, bf16[4,512]{1,0:T(4,128)(2,1)}, u32[]{:S(2)}) copy-start(bf16[4,512]{1,0:T(4,128)(2,1)} %param.20) | copy-start | bytes 12292
  0.0 10.8 %copy-start.17 = (bf16[4,512]{1,0:T(4,128)(2,1)S(1)}, bf16[4,512]{1,0:T(4,128)(2,1)}, u32[]{:S(2)}) copy-start(bf16[4,512]{1,0:T(4,128)(2,1)} %param.21) | copy-start | bytes 12292
  0.0 11.3 %copy-start.11 = (bf16[64,512]{1,0:T(8,128)(2,1)S(1)}, bf16[64,512]{1,0:T(8,128)(2,1)}, u32[]{:S(2)}) copy-start(bf16[64,512]{1,0:T(8,128)(2,1)} %param.16) | copy-start | bytes 196612
  0.0 11.3 %copy-start.12 = (bf16[64,512]{1,0:T(8,128)(2,1)S(1)}, bf16[64,512]{1,0:T(8,128)(2,1)}, u32[]{:S(2)}) copy-start(bf16[64,512]{1,0:T(8,128)(2,1)} %param.17) | copy-start | bytes 196612
  0.1 11.4 %copy-start.9 = (bf16[64,1024]{1,0:T(8,128)(2,1)S(1)}, bf16[64,1024]{1,0:T(8,128)(2,1)}, u32[]{:S(2)}) copy-start(bf16[64,1024]{1,0:T(8,128)(2,1)} %param.15) | copy-start | bytes 393220
  0.1 11.4 %copy-start.10 = (bf16[1024,64]{0,1:T(8,128)(2,1)S(1)}, bf16[1024,64]{0,1:T(8,128)(2,1)}, u32[]{:S(2)}) copy-start(bf16[1024,64]{0,1:T(8,128)(2,1)} %param.25) | copy-start | bytes 393220
  1.0 97.8 %collective-permute-start = (bf16[8,2048]{1,0:T(8,128)(2,1)S(1)}, bf16[8,2048]{1,0:T(8,128)(2,1)S(1)}, u32[]{:S(2)}, u32[]{:S(2)}) collective-permute-start(bf16[8,2048]{1,0:T(8,128)(2,1)S(1)} %slice_bitcast_fusion.3), channel_id=1, source_target_pairs={{0,4},{4,8},{8,12},{12,16},{16,20},{20,24},{24,28},{1,5},{5,9},{9,... | collective-permute-start | bytes 98312 | tf_op jit(solution)/shard_map/ppermute | solution.py:273
  7.8 113.4 %collective-permute-start.2 = (f32[16]{0:T(128)S(1)}, f32[16]{0:T(128)S(1)}, u32[]{:S(2)}, u32[]{:S(2)}) collective-permute-start(f32[16]{0:T(128)S(1)} %get-tuple-element.29), channel_id=1, source_target_pairs={{0,4},{4,8},{8,12},{12,16},{16,20},{20,24},{24,28},{1,5},{5,9},{9,... | collective-permute-start | bytes 200 | tf_op jit(solution)/shard_map/ppermute | solution.py:242
  12.3 86.5 %copy-start.5 = (bf16[1,512,2048]{2,1,0:T(8,128)(2,1)S(1)}, bf16[1,512,2048]{2,1,0:T(8,128)(2,1)}, u32[]{:S(2)}) copy-start(bf16[1,512,2048]{2,1,0:T(8,128)(2,1)} %param.13) | copy-start | bytes 6291460
  117.3 14.7 %copy-start.18 = (f32[1,512]{1,0:T(1,128)S(1)}, f32[1,512]{1,0:T(1,128)}, u32[]{:S(2)}) copy-start(f32[1,512]{1,0:T(1,128)} %get-tuple-element.24) | copy-start | bytes 6148
  119.2 11.4 %collective-permute-start.1 = (bf16[4,4,64,128]{3,2,1,0:T(8,128)(2,1)S(1)}, bf16[4,4,64,128]{3,2,1,0:T(8,128)(2,1)S(1)}, u32[]{:S(2)}, u32[]{:S(2)}) collective-permute-start(bf16[4,4,64,128]{3,2,1,0:T(8,128)(2,1)S(1)} %convert_element_type.105), channel_id=1, source_target_pairs={{0,4},{4,8},{8,12},{12,16},{16,20},{20,24},{24,28},{1,5},{5,9},{9,... | collective-permute-start | bytes 786440 | tf_op jit(solution)/shard_map/ppermute | solution.py:240
  121.2 5.5 %collective-permute-start.4 = (f32[16]{0:T(128)S(1)}, f32[16]{0:T(128)S(1)}, u32[]{:S(2)}, u32[]{:S(2)}) collective-permute-start(f32[16]{0:T(128)S(1)} %get-tuple-element.9), channel_id=1, source_target_pairs={{0,8},{4,12},{8,16},{12,20},{16,24},{20,28},{1,9},{5,13},{9,17},{1... | collective-permute-start | bytes 200 | tf_op jit(solution)/shard_map/ppermute | solution.py:242
  130.7 9.6 %collective-permute-start.3 = (bf16[4,4,64,128]{3,2,1,0:T(8,128)(2,1)S(1)}, bf16[4,4,64,128]{3,2,1,0:T(8,128)(2,1)S(1)}, u32[]{:S(2)}, u32[]{:S(2)}) collective-permute-start(bf16[4,4,64,128]{3,2,1,0:T(8,128)(2,1)S(1)} %fusion.63), channel_id=1, source_target_pairs={{0,8},{4,12},{8,16},{12,20},{16,24},{20,28},{1,9},{5,13},{9,17},{1... | collective-permute-start | bytes 786440 | tf_op jit(solution)/shard_map/ppermute | solution.py:240
  140.5 17.5 %copy-start.3 = (bf16[4,128,4,4,64]{1,0,4,3,2:T(4,128)(2,1)S(1)}, bf16[4,128,4,4,64]{1,0,4,3,2:T(4,128)(2,1)}, u32[]{:S(2)}) copy-start(bf16[4,128,4,4,64]{1,0,4,3,2:T(4,128)(2,1)} %copy-done.2) | copy-start | bytes 3145732
  140.5 17.5 %copy-start.13 = (f32[4,4,4,128]{3,2,1,0:T(4,128)S(1)}, f32[4,4,4,128]{3,2,1,0:T(4,128)}, u32[]{:S(2)}) copy-start(f32[4,4,4,128]{3,2,1,0:T(4,128)} %copy.24) | copy-start | bytes 98308
  140.5 17.5 %copy-start.15 = (pred[128,128]{1,0:T(8,128)(4,1)S(1)}, pred[128,128]{1,0:T(8,128)(4,1)}, u32[]{:S(2)}) copy-start(pred[128,128]{1,0:T(8,128)(4,1)} %iota_compare_fusion) | copy-start | bytes 49156
  140.5 14.4 %collective-permute-start.5 = (bf16[4,4,64,128]{3,2,1,0:T(8,128)(2,1)S(1)}, bf16[4,4,64,128]{3,2,1,0:T(8,128)(2,1)S(1)}, u32[]{:S(2)}, u32[]{:S(2)}) collective-permute-start(bf16[4,4,64,128]{3,2,1,0:T(8,128)(2,1)S(1)} %fusion.67), channel_id=1, source_target_pairs={{0,16},{4,20},{8,24},{12,28},{1,17},{5,21},{9,25},{13,29},{2,18},{... | collective-permute-start | bytes 786440 | tf_op jit(solution)/shard_map/ppermute | solution.py:240
  155.2 11.0 %collective-permute-start.6 = (bf16[4,4,64,128]{3,2,1,0:T(8,128)(2,1)S(1)}, bf16[4,4,64,128]{3,2,1,0:T(8,128)(2,1)S(1)}, u32[]{:S(2)}, u32[]{:S(2)}) collective-permute-start(bf16[4,4,64,128]{3,2,1,0:T(8,128)(2,1)S(1)} %add_convert_fusion), channel_id=1, source_target_pairs={{0,4},{4,8},{8,12},{12,16},{16,20},{20,24},{24,28},{1,5},{5,9},{9,... | collective-permute-start | bytes 786440 | tf_op jit(solution)/shard_map/ppermute | solution.py:245
  158.0 8.2 %copy-start.1 = (f32[4,4,4,64,128]{4,3,2,1,0:T(8,128)S(1)}, f32[4,4,4,64,128]{4,3,2,1,0:T(8,128)}, u32[]{:S(2)}) copy-start(f32[4,4,4,64,128]{4,3,2,1,0:T(8,128)} %get-tuple-element.32) | copy-start | bytes 6291460
  158.1 8.2 %copy-start.19 = (f32[4,4]{1,0:T(4,128)S(1)}, f32[4,4]{1,0:T(4,128)}, u32[]{:S(2)}) copy-start(f32[4,4]{1,0:T(4,128)} %exp.93) | copy-start | bytes 196
  158.1 8.2 %copy-start.20 = (f32[4,4]{1,0:T(4,128)S(1)}, f32[4,4]{1,0:T(4,128)}, u32[]{:S(2)}) copy-start(f32[4,4]{1,0:T(4,128)} %exp.95) | copy-start | bytes 196
  158.1 8.2 %copy-start.21 = (f32[4,4]{1,0:T(4,128)S(1)}, f32[4,4]{1,0:T(4,128)}, u32[]{:S(2)}) copy-start(f32[4,4]{1,0:T(4,128)} %exp.97) | copy-start | bytes 196
  (6 other events, 19.0 us)

commit v2 on v1

--- a/solution.py
+++ b/solution.py
@@ -44,7 +44,22 @@
         pl.when(exists)(action)
 
 
-def gather_kernel(lines, own_ref, full_ref, send_sem, recv_sem, pair_sem, local_sem):
+def gather_kernel(
+    lines,
+    own_ref,
+    tail_ref,
+    span_ref,
+    full_ref,
+    halo_ref,
+    spans_ref,
+    send_sem,
+    recv_sem,
+    pair_sem,
+    local_sem,
+    halo_sem,
+    span_send,
+    span_recv,
+):
     depth, across, along, cores = lines
     sp = lax.axis_index("sp")
     dp = lax.axis_index("dp")
@@ -59,29 +74,59 @@
         return tuple(value if d == dim else here[d] for d in range(3))
 
     barrier = pltpu.get_barrier_semaphore()
-    for dim in range(3):
-        for target, exists in onward(counts[dim], here[dim], here[dim], 0):
-
-            def greet(dim=dim, target=target):
-                pl.semaphore_signal(
-                    barrier,
-                    inc=1,
-                    device_id=target_id(moved(dim, target), core),
-                    device_id_type=pl.DeviceIdType.MESH,
-                )
-
-            when(exists, greet)
+    devices = depth * across
+    peers = devices
+    for step in range(1, devices):
+        pl.semaphore_signal(
+            barrier,
+            inc=1,
+            device_id={"sp": (sp + step) % devices, "dp": dp},
+            device_id_type=pl.DeviceIdType.MESH,
+        )
+    for target, exists in onward(along, here[2], here[2], 0):
+
+        def greet(target=target):
+            pl.semaphore_signal(
+                barrier,
+                inc=1,
+                device_id=target_id(moved(2, target), core),
+                device_id_type=pl.DeviceIdType.MESH,
+            )
+
+        when(exists, greet)
+        peers = peers + (1 if exists is None else jnp.where(exists, 1, 0))
     pl.semaphore_signal(
         barrier,
         inc=1,
         device_id=target_id(here, 1 - core),
         device_id_type=pl.DeviceIdType.MESH,
     )
-    peers = 1
-    for dim in range(3):
-        for target, exists in onward(counts[dim], here[dim], here[dim], 0):
-            peers = peers + (1 if exists is None else jnp.where(exists, 1, 0))
     pl.semaphore_wait(barrier, peers)
+
+    halo_copy = pltpu.make_async_remote_copy(
+        src_ref=tail_ref,
+        dst_ref=halo_ref,
+        send_sem=halo_sem.at[0],
+        recv_sem=halo_sem.at[1],
+        device_id={"sp": (sp + 1) % devices, "dp": dp},
+        device_id_type=pl.DeviceIdType.MESH,
+    )
+    pl.when(sp + 1 < devices)(halo_copy.start)
+    own_span = pltpu.make_async_copy(span_ref, spans_ref.at[sp], halo_sem.at[2])
+    own_span.start()
+
+    def span_copy(step, slot):
+        return pltpu.make_async_remote_copy(
+            src_ref=span_ref,
+            dst_ref=spans_ref.at[slot],
+            send_sem=span_send.at[step - 1],
+            recv_sem=span_recv.at[step - 1],
+            device_id={"sp": (sp + step) % devices, "dp": dp},
+            device_id_type=pl.DeviceIdType.MESH,
+        )
+
+    for step in range(1, devices):
+        span_copy(step, sp).start()
 
     def chip_of(place):
         return (place[0] * across + place[1]) * along + place[2]
@@ -144,9 +189,65 @@
                 device_id_type=pl.DeviceIdType.MESH,
             ).wait_recv()
     local.wait()
-
-
-def gather_rows(own):
+    own_span.wait()
+    for step in range(1, devices):
+        span_copy(step, sp).wait_send()
+        span_copy(step, (sp + devices - step) % devices).wait_recv()
+    pl.when(sp + 1 < devices)(halo_copy.wait_send)
+    pl.when(sp > 0)(halo_copy.wait_recv)
+
+
+def exchange_kernel(devices, in_ref, out_ref, send_sem, recv_sem, local_sem):
+    sp = lax.axis_index("sp")
+    dp = lax.axis_index("dp")
+    barrier = pltpu.get_barrier_semaphore()
+    for step in range(1, devices):
+        pl.semaphore_signal(
+            barrier,
+            inc=1,
+            device_id={"sp": (sp + step) % devices, "dp": dp},
+            device_id_type=pl.DeviceIdType.MESH,
+        )
+    pl.semaphore_wait(barrier, devices - 1)
+
+    def copy(step, slot):
+        target = (sp + step) % devices
+        return pltpu.make_async_remote_copy(
+            src_ref=in_ref.at[target],
+            dst_ref=out_ref.at[slot],
+            send_sem=send_sem.at[step - 1],
+            recv_sem=recv_sem.at[step - 1],
+            device_id={"sp": target, "dp": dp},
+            device_id_type=pl.DeviceIdType.MESH,
+        )
+
+    for step in range(1, devices):
+        copy(step, sp).start()
+    local = pltpu.make_async_copy(in_ref.at[sp], out_ref.at[sp], local_sem)
+    local.start()
+    for step in range(1, devices):
+        copy(step, sp).wait_send()
+        copy(step, (sp + devices - step) % devices).wait_recv()
+    local.wait()
+
+
+def exchange(blocks, identity):
+    devices = blocks.shape[0]
+    return pl.pallas_call(
+        functools.partial(exchange_kernel, devices),
+        out_shape=jax.ShapeDtypeStruct(blocks.shape, blocks.dtype),
+        in_specs=[pl.BlockSpec(memory_space=pltpu.VMEM)],
+        out_specs=pl.BlockSpec(memory_space=pltpu.VMEM),
+        scratch_shapes=[
+            pltpu.SemaphoreType.DMA((devices - 1,)),
+            pltpu.SemaphoreType.DMA((devices - 1,)),
+            pltpu.SemaphoreType.DMA,
+        ],
+        compiler_params=pltpu.CompilerParams(collective_id=identity, has_side_effects=True),
+    )(blocks)
+
+
+def gather_rows(own, tail, span):
     sp, dp = lax.axis_size("sp"), lax.axis_size("dp")
     across = 1
     while 4 * across * across <= sp:
@@ -155,20 +256,31 @@
     chips = sp * dp // 2
     rows, columns = own.shape
     hops = 2 * chips * 7
-    full = pl.pallas_call(
+    full, halo, spans = pl.pallas_call(
         functools.partial(gather_kernel, lines),
-        out_shape=jax.ShapeDtypeStruct((sp * dp, 2, rows // 2, columns), own.dtype),
-        in_specs=[pl.BlockSpec(memory_space=pltpu.VMEM)],
-        out_specs=pl.BlockSpec(memory_space=pl.ANY),
+        out_shape=(
+            jax.ShapeDtypeStruct((sp * dp, 2, rows // 2, columns), own.dtype),
+            jax.ShapeDtypeStruct(tail.shape, tail.dtype),
+            jax.ShapeDtypeStruct((sp,) + span.shape, span.dtype),
+        ),
+        in_specs=[pl.BlockSpec(memory_space=pltpu.VMEM)] * 3,
+        out_specs=(
+            pl.BlockSpec(memory_space=pl.ANY),
+            pl.BlockSpec(memory_space=pltpu.VMEM),
+            pl.BlockSpec(memory_space=pltpu.VMEM),
+        ),
         scratch_shapes=[
             pltpu.SemaphoreType.DMA((hops,)),
             pltpu.SemaphoreType.DMA((chips, 2)),
             pltpu.SemaphoreType.DMA((chips, 2)),
             pltpu.SemaphoreType.DMA,
+            pltpu.SemaphoreType.DMA((3,)),
+            pltpu.SemaphoreType.DMA((sp - 1,)),
+            pltpu.SemaphoreType.DMA((sp - 1,)),
         ],
         compiler_params=pltpu.CompilerParams(collective_id=1, has_side_effects=True),
-    )(own.reshape(2, rows // 2, columns))
-    return full.reshape(sp * dp * rows, columns)
+    )(own.reshape(2, rows // 2, columns), tail, span)
+    return full.reshape(sp * dp * rows, columns), halo, spans
 
 
 def project(rows, weight):
@@ -223,7 +335,7 @@
     return within, states, running, block_reads
 
 
-def entering_states(states, running):
+def entering_states(states, running, spans):
     blocks = states.shape[0]
     share = HEADS // GROUPS
     ends = running[:, -1, :]
@@ -232,17 +344,17 @@
     left = jnp.exp(totals[-1][None] - totals).reshape(blocks, GROUPS, share)
     last = jnp.sum(left[..., None, None] * states, axis=0)
     devices = lax.axis_size("sp")
-    held = last
-    span = totals[-1]
-    stride = 1
-    while stride < devices:
-        pairs = [(i, i + stride) for i in range(devices - stride)]
-        came = lax.ppermute(held.astype(jnp.bfloat16), "sp", pairs).astype(jnp.float32)
-        held = held + jnp.exp(span).reshape(GROUPS, share, 1, 1) * came
-        span = span + lax.ppermute(span, "sp", pairs)
-        stride *= 2
-    pairs = [(i, i + 1) for i in range(devices - 1)]
-    initial = lax.ppermute(held.astype(jnp.bfloat16), "sp", pairs).astype(jnp.float32)
+    held = HEADS // devices
+    came = exchange(last.astype(jnp.bfloat16).reshape(devices, held, HEAD_DIM, STATE), 2)
+    own_spans = lax.dynamic_slice_in_dim(spans, lax.axis_index("sp") * held, held, 1)
+    fades = jnp.exp(own_spans)[:, :, None, None]
+    reached = jnp.zeros(came.shape[1:], jnp.float32)
+    leaving = []
+    for device in range(devices):
+        leaving.append(reached.astype(jnp.bfloat16))
+        reached = reached * fades[device] + came[device].astype(jnp.float32)
+    initial = exchange(jnp.stack(leaving), 3).astype(jnp.float32)
+    initial = initial.reshape(GROUPS, share, HEAD_DIM, STATE)
     current = initial
     entering = []
     for block in range(blocks):
@@ -270,25 +382,27 @@
     sequence = activations[0]
     length = sequence.shape[0]
     devices = lax.axis_size("sp")
-    halo = lax.ppermute(sequence[-8:], "sp", [(i, i + 1) for i in range(devices - 1)])
-    extended = jnp.concatenate([halo, sequence], axis=0)
 
     own = jnp.concatenate(
         [value_weight, input_weight, readout_weight, gate_weight, out_weight.T], axis=1
     )
-    full = gather_rows(own)
+    rate_raw = project(sequence, rate_weight)
+    rates = jax.nn.softplus(rate_raw.astype(jnp.float32) + rate_bias)
+    decay = -jnp.exp(decay_log) / (length * devices)
+    span = jnp.zeros((8, 128), jnp.float32).at[:, :HEADS].set(jnp.sum(rates * decay, axis=0))
+    full, halo, spans = gather_rows(own, sequence[-8:], span)
+    spans = spans[:, 0, :HEADS]
+    halo = jnp.where(lax.axis_index("sp") > 0, halo, jnp.zeros_like(halo))
+    extended = jnp.concatenate([halo, sequence], axis=0)
     ends = [0]
     for weight in (value_weight, input_weight, readout_weight, gate_weight):
         ends.append(ends[-1] + weight.shape[1])
-    rate_raw = project(sequence, rate_weight)
-    rates = jax.nn.softplus(rate_raw.astype(jnp.float32) + rate_bias)
-    decay = -jnp.exp(decay_log) / (length * devices)
     projected = project(extended, full[:, : ends[4]])
     values = halo_conv(projected[:, ends[0] : ends[1]], value_taps, length)
     inputs = halo_conv(projected[:, ends[1] : ends[2]], input_taps, length)
     reads = halo_conv(projected[:, ends[2] : ends[3]], readout_taps, length)
     within, states, running, block_reads = local_mix(values, inputs, reads, rates, decay)
-    entering = entering_states(states, running).astype(jnp.bfloat16)
+    entering = entering_states(states, running, spans).astype(jnp.bfloat16)
     across = jnp.einsum(
         "btgn,bgkpn->btgkp", block_reads, entering, preferred_element_type=jnp.float32
     )

time: 184 us -> 170 us (0.924); the launches traced: 184 us -> 167 us
  waiting for transfers between devices: 34.5 us -> 0 us
  Pallas kernels: 83.8 us -> 107 us
  starting transfers between devices: 14 us -> 0 us
  other arithmetic: 9.32 us -> 20.3 us
  local copies, waits for them, and re-layouts: 18 us -> 15.5 us
    ppermute x7 -> x0, waiting for transfers between devices: 34.5 us -> none  [the longest x4 30.4 us: entering_states(): lax.ppermute(held.astype(jnp.bfloat16), 'sp', pairs).astype(jnp.float32)]
    pallas_call x1 -> x3, Pallas kernels: 83.8 us -> 107 us  [the longest x1 83.5 us: gather_rows(): pl.pallas_call(functools.partial(gather_kernel, lines), out_shape=(jax.Sh...]
    ppermute x7 -> x0, starting transfers between devices: 14 us -> none  [the longest x4 7.44 us: entering_states(): lax.ppermute(held.astype(jnp.bfloat16), 'sp', pairs).astype(jnp.float32)]
    unnamed x0 -> x6, other arithmetic: none -> 5.28 us
    another operation x1 -> x4, other arithmetic: 0.3 us -> 4.2 us  [entering_states(): return jnp.stack(entering)]
  transfers between devices with their start and end apart: 7 -> 0, of which waited for: 5 -> 0; matrix products, arithmetic and copies ran while one was open for 17% -> 0% of each run, Pallas kernels for 46% -> 0%
where the time goes in v2:
time: 170 us; the launch traced here: 167 us
  Pallas kernels  107 us (63%)
  matrix products  24 us (14%)
  other arithmetic  20.3 us (12%)
  local copies, waits for them, and re-layouts  15.5 us (9%)
    pallas_call x1, Pallas kernels, gather_rows(): pl.pallas_call(functools.partial(gather_kernel, lines), out_shape=(jax.Sh...  83.5 us
    pallas_call x2, Pallas kernels, exchange(): pl.pallas_call(functools.partial(exchange_kernel, devices), out_shape=jax...  23.4 us
    dot_general x2, matrix products, project(): jnp.dot(rows, weight, preferred_element_type=jnp.float32)  12.2 us
    convert_element_type x2, local copies, waits for them, and re-layouts, per_device(): mixed.astype(jnp.float32) * jax.nn.silu(gate_proj.astype(jnp.float32))  8.03 us
    dot_general x1, matrix products, per_device(): lax.dot_general(normed, full[:, ends[4]:], (((1,), (1,)), ((), ())), pref...  6.64 us
    unnamed x6, other arithmetic  5.28 us

profile of v2, /device:TPU:24, one launch (start us, length us, event | category | flops | bytes accessed | tf_op | source)
XLA Modules:
  0.0 167.1 jit_solution(6547035801730561879)
XLA Ops:
  0.9 2.4 %multiply_reduce_fusion.2 = (f32[16]{0:T(128)S(1)}, f32[512,16]{0,1:T(8,128)S(1)}) fusion(f32[16]{0:T(128)S(1)} %negate_multiply_fusion, f32[16]{0:T(128)} %param.24, bf16[2048,16]{0,1:T(8,128)(2,1)S(1)} %copy-done, bf16[1,512,2048]{2,1,0:T(8,128)(2,1)} %param.15), kind=kOutput, calls=%fused_computation.111 | convolution fusion | flops 33644528 | bytes 2195648 | tf_op jit(solution)/shard_map/dot_general | solution.py:287
  5.2 0.9 constant_dynamic-update-slice_fusion.3
  7.0 83.5 %shard_map.127 = (bf16[32,2,32,4096]{3,2,1,0:T(8,128)(2,1)}, bf16[8,2048]{1,0:T(8,128)(2,1)}, f32[8,8,128]{2,1,0:T(8,128)}) custom-call(bf16[2,32,4096]{2,1,0:T(8,128)(2,1)} %bitcast.94, bf16[8,2048]{1,0:T(8,128)(2,1)} %slice_bitcast_fusion.tail_ref, f32[8,128]{1,0:T(8,128)} %scatter.8.span_ref), custom_call_target="tpu_custom_call" | custom-call | tf_op jit(solution)/shard_map/pallas_call | solution.py:259
  91.3 9.7 %fusion.2 = bf16[520,3072]{1,0:T(8,128)(2,1)S(1)} fusion(bf16[2048,4096]{1,0:T(8,128)(2,1)} %bitcast.116, bf16[512,2048]{1,0:T(8,128)(2,1)S(1)} %bitcast.92, bf16[8,2048]{1,0:T(8,128)(2,1)S(1)} %broadcast_select_fusion), kind=kOutput, calls=%fused_computation.2 | convolution fusion | flops 6548971520 | bytes 17907712 | tf_op jit(solution)/shard_map/dot_general | solution.py:287
  101.8 2.1 %multiply_convert_fusion.6 = (bf16[512,512]{1,0:T(8,128)(2,1)S(1)}, bf16[512,512]{1,0:T(8,128)(2,1)}) fusion(f32[520,512]{1,0:T(8,128)S(1)} %get-tuple-element.29, f32[512]{0:T(512)S(1)} %bitcast.115, f32[512]{0:T(512)S(1)} %bitcast.114, f32[512]{0:T(512)S(1)} %bitcast.113, f32[512]{0:T(512)S(1)} %bitcast.112, f32[520,512]{1,0:T(8,128)S(1)} %get-tuple-element.28, ...), kind=kLoop, calls=%fused_computation.70 | loop fusion | flops 6291456 | bytes 9453568 | tf_op jit(solution)/shard_map/convert_element_type | solution.py:299
  104.0 1.5 slice_convert_fusion
  105.6 1.3 multiply_convert_fusion.4
  108.7 1.5 multiply_convert_fusion.3
  110.5 2.4 %multiply_reduce_fusion.1 = (bf16[4,4,64,128]{3,2,1,0:T(8,128)(2,1)}, f32[4,4,4,64,128]{4,3,2,1,0:T(8,128)S(1)}) fusion(f32[4,4,4]{2,1,0:T(4,128)S(1)} %bitcast.101, bf16[4,128,4,128,1]{3,2,1,0,4:T(4,128)(2,1)S(1)} %bitcast.89, bf16[4,128,4,4,64]{1,0,4,3,2:T(4,128)(2,1)} %multiply_convert_fusion.3), kind=kOutput, calls=%fused_computation.30 | convolution fusion | flops 135135232 | bytes 3932416 | tf_op jit(solution)/shard_map/bsgkp,bsgn->bgkpn/dot_general | solution.py:332
  112.9 12.2 %shard_map.128 = bf16[8,2,64,128]{3,2,1,0:T(8,128)(2,1)} custom-call(bf16[8,2,64,128]{3,2,1,0:T(8,128)(2,1)} %bitcast.93), custom_call_target="tpu_custom_call" | custom-call | tf_op jit(solution)/shard_map/pallas_call | solution.py:236
  126.9 0.9 fusion.69
  127.7 0.9 convert_dynamic-update-slice_fusion.1
  128.6 0.9 fusion.68
  129.5 0.9 convert_dynamic-update-slice_fusion
  130.5 0.8 fusion.67
  131.3 0.9 fusion.71.in_ref
  132.9 11.2 %shard_map.129 = bf16[8,2,64,128]{3,2,1,0:T(8,128)(2,1)} custom-call(bf16[8,2,64,128]{3,2,1,0:T(8,128)(2,1)} %copy-done.9), custom_call_target="tpu_custom_call" | custom-call | tf_op jit(solution)/shard_map/pallas_call | solution.py:236
  144.5 2.0 %fusion.82 = (bf16[1,4,4,64,128]{4,3,2,1,0:T(8,128)(2,1)S(1)}, bf16[1,4,4,64,128]{4,3,2,1,0:T(8,128)(2,1)}, bf16[1,4,4,64,128]{4,3,2,1,0:T(8,128)(2,1)}) fusion(f32[4,4,4,64,128]{4,3,2,1,0:T(8,128)S(1)} %get-tuple-element.57, f32[4,4]{1,0:T(4,128)S(1)} %exp.84, f32[4,4]{1,0:T(4,128)S(1)} %exp.82, bf16[1,4,4,64,128]{4,3,2,1,0:T(8,128)(2,1)} %bitcast.90, ...), kind=kLoop, calls=%fused_computation.147 | loop fusion | flops 1310720 | bytes 2621632 | tf_op jit(solution)/shard_map/convert.4
  146.6 1.3 reshape.172
  148.4 1.5 fusion.16
  150.5 3.5 %copy.38 = f32[4,128,4,4,64]{4,3,2,1,0:T(4,128)} copy(f32[4,128,4,4,64]{1,4,3,2,0:T(8,128)S(1)} %fusion.32) | data formatting | bytes 4194304 | tf_op jit(solution)/shard_map/convert_element_type | solution.py:413
  154.0 4.5 %reshape.179 = f32[512,1024]{1,0:T(8,128)S(1)} reshape(f32[4,128,4,4,64]{4,3,2,1,0:T(4,128)} %copy.38) | data formatting | bytes 4194304 | tf_op jit(solution)/shard_map/convert_element_type | solution.py:413
  158.5 1.9 %multiply_reduce_fusion = f32[512]{0:T(512)S(1)} fusion(f32[512,1024]{1,0:T(8,128)S(1)} %reshape.179, bf16[520,3072]{1,0:T(8,128)(2,1)} %copy-done.3), kind=kLoop, calls=%fused_computation.29 | loop fusion | flops 4193792 | bytes 3147776 | tf_op jit(solution)/shard_map/reduce_sum | solution.py:414
  160.5 6.6 %fusion.10 = bf16[1,512,2048]{2,1,0:T(8,128)(2,1)} fusion(bf16[2048,4096]{1,0:T(8,128)(2,1)} %bitcast.117, f32[1024]{0:T(1024)S(1)} %copy-done.18, f32[512]{0:T(512)S(1)} %add_rsqrt_fusion, f32[512,1024]{1,0:T(8,128)S(1)} %reshape.179, bf16[520,3072]{1,0:T(8,128)(2,1)} %copy-done.3), kind=kOutput, calls=%fused_computation.7 | convolution fusion | flops 2153250816 | bytes 9443328 | tf_op jit(solution)/shard_map/dot_general | solution.py:416
  (81 shorter events, 11.2 us)
Async XLA Ops:
  0.0 0.9 copy-start
  0.0 6.2 %copy-start.5 = (bf16[1,512,2048]{2,1,0:T(8,128)(2,1)S(1)}, bf16[1,512,2048]{2,1,0:T(8,128)(2,1)}, u32[]{:S(2)}) copy-start(bf16[1,512,2048]{2,1,0:T(8,128)(2,1)} %param.15) | copy-start | bytes 6291460
  0.0 6.1 %copy-start.13 = (bf16[64,512]{1,0:T(8,128)(2,1)S(1)}, bf16[64,512]{1,0:T(8,128)(2,1)}, u32[]{:S(2)}) copy-start(bf16[64,512]{1,0:T(8,128)(2,1)} %param.18) | copy-start | bytes 196612
  0.0 6.1 %copy-start.14 = (bf16[64,512]{1,0:T(8,128)(2,1)S(1)}, bf16[64,512]{1,0:T(8,128)(2,1)}, u32[]{:S(2)}) copy-start(bf16[64,512]{1,0:T(8,128)(2,1)} %param.19) | copy-start | bytes 196612
  0.0 6.1 %copy-start.11 = (bf16[64,1024]{1,0:T(8,128)(2,1)S(1)}, bf16[64,1024]{1,0:T(8,128)(2,1)}, u32[]{:S(2)}) copy-start(bf16[64,1024]{1,0:T(8,128)(2,1)} %param.17) | copy-start | bytes 393220
  0.0 6.1 %copy-start.12 = (bf16[1024,64]{0,1:T(8,128)(2,1)S(1)}, bf16[1024,64]{0,1:T(8,128)(2,1)}, u32[]{:S(2)}) copy-start(bf16[1024,64]{0,1:T(8,128)(2,1)} %param.27) | copy-start | bytes 393220
  6.2 0.8 copy-start.8
  101.0 2.9 %copy-start.3 = (bf16[520,3072]{1,0:T(8,128)(2,1)}, bf16[520,3072]{1,0:T(8,128)(2,1)S(1)}, u32[]{:S(2)}) copy-start(bf16[520,3072]{1,0:T(8,128)(2,1)S(1)} %fusion.2) | copy-start | bytes 9584644
  101.0 0.7 copy-start.16
  101.1 0.8 copy-start.17
  103.9 1.6 copy-start.15
  107.7 2.8 %copy-start.1 = (bf16[4,128,4,4,64]{1,0,4,3,2:T(4,128)(2,1)}, bf16[4,128,4,4,64]{1,0,4,3,2:T(4,128)(2,1)S(1)}, u32[]{:S(2)}) copy-start(bf16[4,128,4,4,64]{1,0,4,3,2:T(4,128)(2,1)S(1)} %reshape.171) | copy-start | bytes 3145732
  132.2 0.7 copy-start.9
  146.6 1.8 %copy-start.2 = (bf16[4,128,4,4,64]{1,0,4,3,2:T(4,128)(2,1)S(1)}, bf16[4,128,4,4,64]{1,0,4,3,2:T(4,128)(2,1)}, u32[]{:S(2)}) copy-start(bf16[4,128,4,4,64]{1,0,4,3,2:T(4,128)(2,1)} %copy-done.1) | copy-start | bytes 3145732
  148.4 1.6 copy-start.4
  148.4 1.6 copy-start.6
  148.4 1.6 copy-start.7
  148.4 1.6 copy-start.10
  158.5 2.0 %copy-start.18 = (f32[1024]{0:T(1024)S(1)}, f32[1024]{0:T(1024)}, u32[]{:S(2)}) copy-start(f32[1024]{0:T(1024)} %param.26) | copy-start | bytes 12292

commit v3 on v2

--- a/solution.py
+++ b/solution.py
@@ -13,6 +13,8 @@
 GROUPS = 4
 STATE = 128
 BLOCK = 128
+LAG = 2
+TILE = 512
 
 
 norm_eps = 1.0
@@ -49,17 +51,23 @@
     own_ref,
     tail_ref,
     span_ref,
-    full_ref,
-    halo_ref,
-    spans_ref,
-    send_sem,
-    recv_sem,
-    pair_sem,
-    local_sem,
-    halo_sem,
-    span_send,
-    span_recv,
+    *rest,
 ):
+    fused = len(rest) > 10
+    if fused:
+        seq_ref, proj_ref, outw_ref, spans_ref = rest[:4]
+        full_ref, halo_ref, ext_ref, acc_ref, out_sem = rest[4:9]
+    else:
+        full_ref, halo_ref, spans_ref = rest[:3]
+    (
+        send_sem,
+        recv_sem,
+        pair_sem,
+        local_sem,
+        halo_sem,
+        span_send,
+        span_recv,
+    ) = rest[-7:]
     depth, across, along, cores = lines
     sp = lax.axis_index("sp")
     dp = lax.axis_index("dp")
@@ -137,7 +145,62 @@
     ranks = sorted(itertools.product(*(range(n) for n in counts)), key=lambda r: (sum(r), r))
     used = 0
     started = []
-    arrivals = []
+    chips = []
+
+    def wait_pair(chip):
+        for half in range(2):
+            landed = full_ref.at[chip * cores + 1 - core, half]
+            pltpu.make_async_remote_copy(
+                src_ref=landed,
+                dst_ref=landed,
+                send_sem=send_sem.at[0],
+                recv_sem=pair_sem.at[chip, half],
+                device_id=target_id(here, 1 - core),
+                device_id_type=pl.DeviceIdType.MESH,
+            ).wait_recv()
+
+    def out_copy(chip):
+        width = proj_ref.shape[1]
+        return pltpu.make_async_copy(
+            full_ref.at[pl.ds(chip * cores, cores), :, :, pl.ds(width, outw_ref.shape[3])],
+            outw_ref.at[pl.ds(chip * cores, cores)],
+            out_sem.at[chip],
+        )
+
+    def accumulate(event):
+        chip = chips[event]
+        if event == 0:
+            local.wait()
+            lead = halo_ref.shape[0]
+
+            def take():
+                halo_copy.wait_recv()
+                ext_ref[:lead] = halo_ref[...]
+
+            def clear():
+                ext_ref[:lead] = jnp.zeros_like(halo_ref)
+
+            pl.when(sp > 0)(take)
+            pl.when(sp == 0)(clear)
+        wait_pair(chip)
+        out_copy(chip).start()
+        depth_rows = cores * 2 * full_ref.shape[2]
+        rows = ext_ref[:, pl.ds(pl.multiple_of(chip * depth_rows, 128), depth_rows)]
+
+        def tile(index, carry):
+            columns = pl.ds(pl.multiple_of(index * TILE, TILE), TILE)
+            piece = full_ref[pl.ds(chip * cores, cores), :, :, columns].reshape(depth_rows, TILE)
+            product = jnp.dot(rows, piece, preferred_element_type=jnp.float32)
+            if event == 0:
+                acc_ref[:, columns] = product
+            elif event == len(ranks) - 1:
+                proj_ref[:, columns] = (acc_ref[:, columns] + product).astype(proj_ref.dtype)
+            else:
+                acc_ref[:, columns] += product
+            return carry
+
+        lax.fori_loop(0, proj_ref.shape[1] // TILE, tile, 0)
+
     for rank in ranks:
         origin = tuple(nearest(counts[d], here[d], rank[d]) for d in range(3))
         chip = chip_of(origin)
@@ -175,26 +238,29 @@
                 used += 1
                 when(exists, copy.start)
                 started.append((copy, exists))
+        chips.append(chip)
+        if fused and len(chips) == 1:
+            ext_ref[halo_ref.shape[0] :] = seq_ref[...]
+        if fused and len(chips) > LAG:
+            accumulate(len(chips) - 1 - LAG)
+    if fused:
+        for event in range(len(chips) - LAG, len(chips)):
+            accumulate(event)
     for copy, exists in started:
         when(exists, copy.wait_send)
     for chip in range(depth * across * along):
-        for half in range(2):
-            landed = full_ref.at[chip * cores + 1 - core, half]
-            pltpu.make_async_remote_copy(
-                src_ref=landed,
-                dst_ref=landed,
-                send_sem=send_sem.at[0],
-                recv_sem=pair_sem.at[chip, half],
-                device_id=target_id(here, 1 - core),
-                device_id_type=pl.DeviceIdType.MESH,
-            ).wait_recv()
-    local.wait()
+        if fused:
+            out_copy(chip).wait()
+        else:
+            wait_pair(chip)
+    if not fused:
+        local.wait()
+        pl.when(sp > 0)(halo_copy.wait_recv)
     own_span.wait()
     for step in range(1, devices):
         span_copy(step, sp).wait_send()
         span_copy(step, (sp + devices - step) % devices).wait_recv()
     pl.when(sp + 1 < devices)(halo_copy.wait_send)
-    pl.when(sp > 0)(halo_copy.wait_recv)
 
 
 def exchange_kernel(devices, in_ref, out_ref, send_sem, recv_sem, local_sem):
@@ -245,6 +311,50 @@
         ],
         compiler_params=pltpu.CompilerParams(collective_id=identity, has_side_effects=True),
     )(blocks)
+
+
+def gather_project(own, tail, span, sequence, width):
+    sp, dp = lax.axis_size("sp"), lax.axis_size("dp")
+    rows, columns = own.shape
+    if 2 * rows % 128 or width % TILE:
+        full, halo, spans = gather_rows(own, tail, span)
+        halo = jnp.where(lax.axis_index("sp") > 0, halo, jnp.zeros_like(halo))
+        extended = jnp.concatenate([halo, sequence], axis=0)
+        return project(extended, full[:, :width]), full[:, width:], spans
+    across = 1
+    while 4 * across * across <= sp:
+        across *= 2
+    lines = (sp // across, across, dp // 2, 2)
+    chips = sp * dp // 2
+    length, model = sequence.shape
+    lead = tail.shape[0]
+    vmem = pl.BlockSpec(memory_space=pltpu.VMEM)
+    projected, outw, spans = pl.pallas_call(
+        functools.partial(gather_kernel, lines),
+        out_shape=(
+            jax.ShapeDtypeStruct((lead + length, width), own.dtype),
+            jax.ShapeDtypeStruct((sp * dp, 2, rows // 2, columns - width), own.dtype),
+            jax.ShapeDtypeStruct((sp,) + span.shape, span.dtype),
+        ),
+        in_specs=[vmem] * 4,
+        out_specs=(vmem, pl.BlockSpec(memory_space=pl.ANY), vmem),
+        scratch_shapes=[
+            pltpu.VMEM((sp * dp, 2, rows // 2, columns), own.dtype),
+            pltpu.VMEM(tail.shape, tail.dtype),
+            pltpu.VMEM((lead + length, model), sequence.dtype),
+            pltpu.VMEM((lead + length, width), jnp.float32),
+            pltpu.SemaphoreType.DMA((chips,)),
+            pltpu.SemaphoreType.DMA((2 * chips * 7,)),
+            pltpu.SemaphoreType.DMA((chips, 2)),
+            pltpu.SemaphoreType.DMA((chips, 2)),
+            pltpu.SemaphoreType.DMA,
+            pltpu.SemaphoreType.DMA((3,)),
+            pltpu.SemaphoreType.DMA((sp - 1,)),
+            pltpu.SemaphoreType.DMA((sp - 1,)),
+        ],
+        compiler_params=pltpu.CompilerParams(collective_id=1, has_side_effects=True),
+    )(own.reshape(2, rows // 2, columns), tail, span, sequence)
+    return projected, outw.reshape(sp * dp * rows, columns - width), spans
 
 
 def gather_rows(own, tail, span):
@@ -390,14 +500,12 @@
     rates = jax.nn.softplus(rate_raw.astype(jnp.float32) + rate_bias)
     decay = -jnp.exp(decay_log) / (length * devices)
     span = jnp.zeros((8, 128), jnp.float32).at[:, :HEADS].set(jnp.sum(rates * decay, axis=0))
-    full, halo, spans = gather_rows(own, sequence[-8:], span)
-    spans = spans[:, 0, :HEADS]
-    halo = jnp.where(lax.axis_index("sp") > 0, halo, jnp.zeros_like(halo))
-    extended = jnp.concatenate([halo, sequence], axis=0)
     ends = [0]
     for weight in (value_weight, input_weight, readout_weight, gate_weight):
         ends.append(ends[-1] + weight.shape[1])
-    projected = project(extended, full[:, : ends[4]])
+    lead = 16
+    projected, out_full, spans = gather_project(own, sequence[-lead:], span, sequence, ends[4])
+    spans = spans[:, 0, :HEADS]
     values = halo_conv(projected[:, ends[0] : ends[1]], value_taps, length)
     inputs = halo_conv(projected[:, ends[1] : ends[2]], input_taps, length)
     reads = halo_conv(projected[:, ends[2] : ends[3]], readout_taps, length)
@@ -409,12 +517,12 @@
     fade = jnp.exp(running).reshape(across.shape[:4])
     mixed = (within + across * fade[..., None]).reshape(length, HEADS * HEAD_DIM)
     mixed = mixed.astype(jnp.bfloat16)
-    gate_proj = projected[halo.shape[0] :, ends[3] : ends[4]]
+    gate_proj = projected[lead:, ends[3] : ends[4]]
     gated = mixed.astype(jnp.float32) * jax.nn.silu(gate_proj.astype(jnp.float32))
     scale = lax.rsqrt(jnp.mean(gated * gated, axis=-1, keepdims=True) + norm_eps)
     normed = (gated * scale * norm_gain).astype(jnp.bfloat16)
     result = lax.dot_general(
-        normed, full[:, ends[4] :], (((1,), (1,)), ((), ())), preferred_element_type=jnp.float32
+        normed, out_full, (((1,), (1,)), ((), ())), preferred_element_type=jnp.float32
     )
     return result.astype(jnp.bfloat16)[None]
 

time: 170 us -> 166 us (0.976)
  matrix products: 24 us -> 14.2 us
  Pallas kernels: 107 us -> 113 us
    dot_general x2 -> x1, matrix products: 12.2 us -> 2.38 us  [project(): jnp.dot(rows, weight, preferred_element_type=jnp.float32)]
    pallas_call x1, Pallas kernels: 83.5 us -> 92.9 us  [gather_project(): pl.pallas_call(functools.partial(gather_kernel, lines), out_shape=(jax.Sh...]
    pallas_call x2, Pallas kernels: 23.4 us -> 19.7 us  [exchange(): pl.pallas_call(functools.partial(exchange_kernel, devices), out_shape=jax...]
where the time goes in v3:
time: 166 us; the launch traced here: 163 us
  Pallas kernels  113 us (68%)
  other arithmetic  20.7 us (12%)
  local copies, waits for them, and re-layouts  14.8 us (9%)
  matrix products  14.2 us (9%)
    pallas_call x1, Pallas kernels, gather_project(): pl.pallas_call(functools.partial(gather_kernel, lines), out_shape=(jax.Sh...  92.9 us
    pallas_call x2, Pallas kernels, exchange(): pl.pallas_call(functools.partial(exchange_kernel, devices), out_shape=jax...  19.7 us
    convert_element_type x2, local copies, waits for them, and re-layouts, per_device(): mixed.astype(jnp.float32) * jax.nn.silu(gate_proj.astype(jnp.float32))  7.84 us
    dot_general x1, matrix products, per_device(): lax.dot_general(normed, out_full, (((1,), (1,)), ((), ())), preferred_ele...  6.64 us
    unnamed x6, other arithmetic  5.28 us
    convert_element_type x2, other arithmetic, halo_conv(): return jax.nn.silu(result).astype(jnp.bfloat16)  3.36 us
    another operation x3, other arithmetic  3.35 us

profile of v3, /device:TPU:24, one launch (start us, length us, event | category | flops | bytes accessed | tf_op | source)
XLA Modules:
  0.0 162.8 jit_solution(8497765111711255479)
XLA Ops:
  0.8 2.4 %multiply_reduce_fusion.2 = (f32[16]{0:T(128)S(1)}, f32[512,16]{0,1:T(8,128)S(1)}) fusion(f32[16]{0:T(128)S(1)} %negate_multiply_fusion, f32[16]{0:T(128)} %param.24, bf16[2048,16]{0,1:T(8,128)(2,1)S(1)} %copy-done, bf16[1,512,2048]{2,1,0:T(8,128)(2,1)} %param.15), kind=kOutput, calls=%fused_computation.104 | convolution fusion | flops 33644528 | bytes 2195648 | tf_op jit(solution)/shard_map/dot_general | solution.py:397
  5.3 1.5 slice_bitcast_fusion.tail_ref
  6.8 92.9 %shard_map.127 = (bf16[528,3072]{1,0:T(8,128)(2,1)}, bf16[32,2,32,1024]{3,2,1,0:T(8,128)(2,1)}, f32[8,8,128]{2,1,0:T(8,128)}) custom-call(bf16[2,32,4096]{2,1,0:T(8,128)(2,1)} %bitcast.95, bf16[16,2048]{1,0:T(8,128)(2,1)} %slice_bitcast_fusion.tail_ref, f32[8,128]{1,0:T(8,128)} %scatter.8.span_ref, bf16[512,2048]{1,0:T(8,128)(2,1)} %bitcast.90), custom_call_target="tpu_custom_call" | custom-call | tf_op jit(solution)/shard_map/pallas_call | solution.py:332
  99.7 1.5 slice_convert_fusion.2
  101.3 2.1 %multiply_convert_fusion.6 = (bf16[512,512]{1,0:T(8,128)(2,1)S(1)}, bf16[512,512]{1,0:T(8,128)(2,1)}) fusion(f32[528,512]{1,0:T(8,128)S(1)} %get-tuple-element.29, f32[512]{0:T(512)S(1)} %bitcast.116, f32[512]{0:T(512)S(1)} %bitcast.115, f32[512]{0:T(512)S(1)} %bitcast.114, f32[512]{0:T(512)S(1)} %bitcast.113, f32[528,512]{1,0:T(8,128)S(1)} %get-tuple-element.28, ...), kind=kLoop, calls=%fused_computation.62 | loop fusion | flops 6291456 | bytes 9453568 | tf_op jit(solution)/shard_map/convert_element_type | solution.py:409
  104.5 1.5 slice_convert_fusion
  106.1 1.3 multiply_convert_fusion.4
  108.2 1.5 multiply_convert_fusion.3
  109.9 2.5 %multiply_reduce_fusion.1 = (bf16[4,4,64,128]{3,2,1,0:T(8,128)(2,1)}, f32[4,4,4,64,128]{4,3,2,1,0:T(8,128)S(1)}) fusion(f32[4,4,4]{2,1,0:T(4,128)S(1)} %bitcast.102, bf16[4,128,4,128,1]{3,2,1,0,4:T(4,128)(2,1)S(1)} %bitcast.91, bf16[4,128,4,4,64]{1,0,4,3,2:T(4,128)(2,1)} %multiply_convert_fusion.3), kind=kOutput, calls=%fused_computation.22 | convolution fusion | flops 135135232 | bytes 3932416 | tf_op jit(solution)/shard_map/bsgkp,bsgn->bgkpn/dot_general | solution.py:442
  112.4 9.9 %shard_map.128 = bf16[8,2,64,128]{3,2,1,0:T(8,128)(2,1)} custom-call(bf16[8,2,64,128]{3,2,1,0:T(8,128)(2,1)} %bitcast.94), custom_call_target="tpu_custom_call" | custom-call | tf_op jit(solution)/shard_map/pallas_call | solution.py:302
  124.0 0.9 fusion.54
  124.9 0.9 convert_dynamic-update-slice_fusion.1
  125.8 0.9 fusion.53
  126.7 0.9 convert_dynamic-update-slice_fusion
  127.6 0.8 fusion.52
  128.5 0.9 fusion.56.in_ref
  130.0 9.8 %shard_map.129 = bf16[8,2,64,128]{3,2,1,0:T(8,128)(2,1)} custom-call(bf16[8,2,64,128]{3,2,1,0:T(8,128)(2,1)} %copy-done.7), custom_call_target="tpu_custom_call" | custom-call | tf_op jit(solution)/shard_map/pallas_call | solution.py:302
  140.3 2.1 %fusion.66 = (bf16[1,4,4,64,128]{4,3,2,1,0:T(8,128)(2,1)S(1)}, bf16[1,4,4,64,128]{4,3,2,1,0:T(8,128)(2,1)}, bf16[1,4,4,64,128]{4,3,2,1,0:T(8,128)(2,1)}) fusion(f32[4,4,4,64,128]{4,3,2,1,0:T(8,128)S(1)} %get-tuple-element.57, f32[4,4]{1,0:T(4,128)S(1)} %exp.84, f32[4,4]{1,0:T(4,128)S(1)} %exp.82, bf16[1,4,4,64,128]{4,3,2,1,0:T(8,128)(2,1)} %bitcast.92, ...), kind=kLoop, calls=%fused_computation.137 | loop fusion | flops 1310720 | bytes 2621632 | tf_op jit(solution)/shard_map/convert.4
  142.4 1.3 reshape.171
  144.2 1.5 fusion.1
  146.3 3.3 %copy.38 = f32[4,128,4,4,64]{4,3,2,1,0:T(4,128)} copy(f32[4,128,4,4,64]{1,4,3,2,0:T(8,128)S(1)} %fusion.17) | data formatting | bytes 4194304 | tf_op jit(solution)/shard_map/convert_element_type | solution.py:521
  149.6 4.5 %reshape.179 = f32[512,1024]{1,0:T(8,128)S(1)} reshape(f32[4,128,4,4,64]{4,3,2,1,0:T(4,128)} %copy.38) | data formatting | bytes 4194304 | tf_op jit(solution)/shard_map/convert_element_type | solution.py:521
  154.2 1.9 %multiply_reduce_fusion = f32[512]{0:T(512)S(1)} fusion(f32[512,1024]{1,0:T(8,128)S(1)} %reshape.179, bf16[528,3072]{1,0:T(8,128)(2,1)} %get-tuple-element.20), kind=kLoop, calls=%fused_computation.21 | loop fusion | flops 4193792 | bytes 3147776 | tf_op jit(solution)/shard_map/reduce_sum | solution.py:522
  156.1 6.6 %fusion = bf16[1,512,2048]{2,1,0:T(8,128)(2,1)} fusion(bf16[2048,1024]{1,0:T(8,128)(2,1)} %bitcast.117, f32[1024]{0:T(1024)S(1)} %copy-done.17, f32[512]{0:T(512)S(1)} %add_rsqrt_fusion, f32[512,1024]{1,0:T(8,128)S(1)} %reshape.179, bf16[528,3072]{1,0:T(8,128)(2,1)} %get-tuple-element.20), kind=kOutput, calls=%fused_computation.2 | convolution fusion | flops 2153250816 | bytes 9443328 | tf_op jit(solution)/shard_map/dot_general | solution.py:524
  (77 shorter events, 8.9 us)
Async XLA Ops:
  0.0 0.8 copy-start
  0.0 5.1 %copy-start.9 = (bf16[64,1024]{1,0:T(8,128)(2,1)S(1)}, bf16[64,1024]{1,0:T(8,128)(2,1)}, u32[]{:S(2)}) copy-start(bf16[64,1024]{1,0:T(8,128)(2,1)} %param.16) | copy-start | bytes 393220
  0.0 5.1 %copy-start.12 = (bf16[64,512]{1,0:T(8,128)(2,1)S(1)}, bf16[64,512]{1,0:T(8,128)(2,1)}, u32[]{:S(2)}) copy-start(bf16[64,512]{1,0:T(8,128)(2,1)} %param.18) | copy-start | bytes 196612
  0.0 5.2 %copy-start.13 = (bf16[64,512]{1,0:T(8,128)(2,1)S(1)}, bf16[64,512]{1,0:T(8,128)(2,1)}, u32[]{:S(2)}) copy-start(bf16[64,512]{1,0:T(8,128)(2,1)} %param.19) | copy-start | bytes 196612
  0.0 5.2 %copy-start.10 = (bf16[64,1024]{1,0:T(8,128)(2,1)S(1)}, bf16[64,1024]{1,0:T(8,128)(2,1)}, u32[]{:S(2)}) copy-start(bf16[64,1024]{1,0:T(8,128)(2,1)} %param.17) | copy-start | bytes 393220
  0.0 5.2 %copy-start.11 = (bf16[1024,64]{0,1:T(8,128)(2,1)S(1)}, bf16[1024,64]{0,1:T(8,128)(2,1)}, u32[]{:S(2)}) copy-start(bf16[1024,64]{0,1:T(8,128)(2,1)} %param.27) | copy-start | bytes 393220
  5.2 1.6 copy-start.6
  99.7 1.5 copy-start.15
  99.7 1.6 copy-start.16
  103.4 2.7 %copy-start.14 = (bf16[4,1024]{1,0:T(4,128)(2,1)S(1)}, bf16[4,1024]{1,0:T(4,128)(2,1)}, u32[]{:S(2)}) copy-start(bf16[4,1024]{1,0:T(4,128)(2,1)} %param.21) | copy-start | bytes 24580
  108.2 1.7 %copy-start.1 = (bf16[4,128,4,4,64]{1,0,4,3,2:T(4,128)(2,1)}, bf16[4,128,4,4,64]{1,0,4,3,2:T(4,128)(2,1)S(1)}, u32[]{:S(2)}) copy-start(bf16[4,128,4,4,64]{1,0,4,3,2:T(4,128)(2,1)S(1)} %reshape.170) | copy-start | bytes 3145732
  129.3 0.7 copy-start.7
  142.4 1.8 %copy-start.2 = (bf16[4,128,4,4,64]{1,0,4,3,2:T(4,128)(2,1)S(1)}, bf16[4,128,4,4,64]{1,0,4,3,2:T(4,128)(2,1)}, u32[]{:S(2)}) copy-start(bf16[4,128,4,4,64]{1,0,4,3,2:T(4,128)(2,1)} %copy-done.1) | copy-start | bytes 3145732
  144.2 1.6 copy-start.3
  144.2 1.6 copy-start.4
  144.2 1.6 copy-start.5
  144.2 1.6 copy-start.8
  154.2 2.0 %copy-start.17 = (f32[1024]{0:T(1024)S(1)}, f32[1024]{0:T(1024)}, u32[]{:S(2)}) copy-start(f32[1024]{0:T(1024)} %param.26) | copy-start | bytes 12292

commit v4 on v3

--- a/solution.py
+++ b/solution.py
@@ -263,7 +263,9 @@
     pl.when(sp + 1 < devices)(halo_copy.wait_send)
 
 
-def exchange_kernel(devices, in_ref, out_ref, send_sem, recv_sem, local_sem):
+def scan_kernel(
+    devices, in_ref, fade_ref, out_ref, came_ref, leave_ref, send_sem, recv_sem, local_sem
+):
     sp = lax.axis_index("sp")
     dp = lax.axis_index("dp")
     barrier = pltpu.get_barrier_semaphore()
@@ -276,41 +278,51 @@
         )
     pl.semaphore_wait(barrier, devices - 1)
 
-    def copy(step, slot):
-        target = (sp + step) % devices
-        return pltpu.make_async_remote_copy(
-            src_ref=in_ref.at[target],
-            dst_ref=out_ref.at[slot],
-            send_sem=send_sem.at[step - 1],
-            recv_sem=recv_sem.at[step - 1],
-            device_id={"sp": target, "dp": dp},
-            device_id_type=pl.DeviceIdType.MESH,
-        )
-
-    for step in range(1, devices):
-        copy(step, sp).start()
-    local = pltpu.make_async_copy(in_ref.at[sp], out_ref.at[sp], local_sem)
-    local.start()
-    for step in range(1, devices):
-        copy(step, sp).wait_send()
-        copy(step, (sp + devices - step) % devices).wait_recv()
-    local.wait()
-
-
-def exchange(blocks, identity):
+    def exchange(phase, from_ref, to_ref):
+        def copy(step, slot):
+            target = (sp + step) % devices
+            return pltpu.make_async_remote_copy(
+                src_ref=from_ref.at[target],
+                dst_ref=to_ref.at[slot],
+                send_sem=send_sem.at[phase, step - 1],
+                recv_sem=recv_sem.at[phase, step - 1],
+                device_id={"sp": target, "dp": dp},
+                device_id_type=pl.DeviceIdType.MESH,
+            )
+
+        for step in range(1, devices):
+            copy(step, sp).start()
+        local = pltpu.make_async_copy(from_ref.at[sp], to_ref.at[sp], local_sem.at[phase])
+        local.start()
+        for step in range(1, devices):
+            copy(step, sp).wait_send()
+            copy(step, (sp + devices - step) % devices).wait_recv()
+        local.wait()
+
+    exchange(0, in_ref, came_ref)
+    reached = jnp.zeros(came_ref.shape[1:], jnp.float32)
+    for device in range(devices):
+        leave_ref[device] = reached.astype(leave_ref.dtype)
+        reached = reached * fade_ref[device] + came_ref[device].astype(jnp.float32)
+    exchange(1, leave_ref, out_ref)
+
+
+def scan_states(blocks, fades):
     devices = blocks.shape[0]
     return pl.pallas_call(
-        functools.partial(exchange_kernel, devices),
+        functools.partial(scan_kernel, devices),
         out_shape=jax.ShapeDtypeStruct(blocks.shape, blocks.dtype),
-        in_specs=[pl.BlockSpec(memory_space=pltpu.VMEM)],
+        in_specs=[pl.BlockSpec(memory_space=pltpu.VMEM)] * 2,
         out_specs=pl.BlockSpec(memory_space=pltpu.VMEM),
         scratch_shapes=[
-            pltpu.SemaphoreType.DMA((devices - 1,)),
-            pltpu.SemaphoreType.DMA((devices - 1,)),
-            pltpu.SemaphoreType.DMA,
+            pltpu.VMEM(blocks.shape, blocks.dtype),
+            pltpu.VMEM(blocks.shape, blocks.dtype),
+            pltpu.SemaphoreType.DMA((2, devices - 1)),
+            pltpu.SemaphoreType.DMA((2, devices - 1)),
+            pltpu.SemaphoreType.DMA((2,)),
         ],
-        compiler_params=pltpu.CompilerParams(collective_id=identity, has_side_effects=True),
-    )(blocks)
+        compiler_params=pltpu.CompilerParams(collective_id=2, has_side_effects=True),
+    )(blocks, fades)
 
 
 def gather_project(own, tail, span, sequence, width):
@@ -455,15 +467,10 @@
     last = jnp.sum(left[..., None, None] * states, axis=0)
     devices = lax.axis_size("sp")
     held = HEADS // devices
-    came = exchange(last.astype(jnp.bfloat16).reshape(devices, held, HEAD_DIM, STATE), 2)
     own_spans = lax.dynamic_slice_in_dim(spans, lax.axis_index("sp") * held, held, 1)
-    fades = jnp.exp(own_spans)[:, :, None, None]
-    reached = jnp.zeros(came.shape[1:], jnp.float32)
-    leaving = []
-    for device in range(devices):
-        leaving.append(reached.astype(jnp.bfloat16))
-        reached = reached * fades[device] + came[device].astype(jnp.float32)
-    initial = exchange(jnp.stack(leaving), 3).astype(jnp.float32)
+    fades = jnp.broadcast_to(jnp.exp(own_spans)[:, :, None, None], (devices, held, 1, STATE))
+    packed = last.astype(jnp.bfloat16).reshape(devices, held, HEAD_DIM, STATE)
+    initial = scan_states(packed, fades).astype(jnp.float32)
     initial = initial.reshape(GROUPS, share, HEAD_DIM, STATE)
     current = initial
     entering = []

time: 166 us -> 157 us (0.946)
  other arithmetic: 20.7 us -> 14.5 us
  Pallas kernels: 113 us -> 110 us
    unnamed x6 -> x0, other arithmetic: 5.28 us -> none
    pallas_call x2 -> x1, Pallas kernels: 19.7 us -> 16.5 us  [scan_states(): pl.pallas_call(functools.partial(scan_kernel, devices), out_shape=jax.Sha...]
    another operation x4 -> x3, other arithmetic: 4.21 us -> 3.34 us
where the time goes in v4:
time: 157 us; the launch traced here: 154 us
  Pallas kernels  110 us (70%)
  local copies, waits for them, and re-layouts  14.8 us (9%)
  other arithmetic  14.5 us (9%)
  matrix products  14.2 us (9%)
    pallas_call x1, Pallas kernels, gather_project(): pl.pallas_call(functools.partial(gather_kernel, lines), out_shape=(jax.Sh...  93.2 us
    pallas_call x1, Pallas kernels, scan_states(): pl.pallas_call(functools.partial(scan_kernel, devices), out_shape=jax.Sha...  16.5 us
    convert_element_type x2, local copies, waits for them, and re-layouts, per_device(): mixed.astype(jnp.float32) * jax.nn.silu(gate_proj.astype(jnp.float32))  7.84 us
    dot_general x1, matrix products, per_device(): lax.dot_general(normed, out_full, (((1,), (1,)), ((), ())), preferred_ele...  6.64 us
    convert_element_type x2, other arithmetic, halo_conv(): return jax.nn.silu(result).astype(jnp.bfloat16)  3.35 us
    another operation x3, other arithmetic  3.34 us

profile of v4, /device:TPU:24, one launch (start us, length us, event | category | flops | bytes accessed | tf_op | source)
XLA Modules:
  0.0 153.6 jit_solution(13912510142736884190)
XLA Ops:
  0.0 0.7 negate_multiply_fusion
  0.8 2.4 %multiply_reduce_fusion.2 = (f32[16]{0:T(128)S(1)}, f32[512,16]{0,1:T(8,128)S(1)}) fusion(f32[16]{0:T(128)S(1)} %negate_multiply_fusion, f32[16]{0:T(128)} %param.24, bf16[2048,16]{0,1:T(8,128)(2,1)S(1)} %copy-done, bf16[1,512,2048]{2,1,0:T(8,128)(2,1)} %param.15), kind=kOutput, calls=%fused_computation.85 | convolution fusion | flops 33644528 | bytes 2195648 | tf_op jit(solution)/shard_map/dot_general | solution.py:409
  3.2 0.6 compare_reduce_fusion
  3.9 0.6 broadcast_select_fusion
  4.5 0.6 scatter.8.span_ref
  5.3 1.6 %slice_bitcast_fusion.tail_ref = bf16[16,2048]{1,0:T(8,128)(2,1)} fusion(bf16[1,512,2048]{2,1,0:T(8,128)(2,1)} %param.15), kind=kLoop, calls=%fused_computation.79 | loop fusion | bytes 131072 | tf_op jit(solution)/shard_map/slice | solution.py:514
  6.8 93.2 %shard_map.127 = (bf16[528,3072]{1,0:T(8,128)(2,1)}, bf16[32,2,32,1024]{3,2,1,0:T(8,128)(2,1)}, f32[8,8,128]{2,1,0:T(8,128)}) custom-call(bf16[2,32,4096]{2,1,0:T(8,128)(2,1)} %bitcast.79, bf16[16,2048]{1,0:T(8,128)(2,1)} %slice_bitcast_fusion.tail_ref, f32[8,128]{1,0:T(8,128)} %scatter.8.span_ref, bf16[512,2048]{1,0:T(8,128)(2,1)} %bitcast.73), custom_call_target="tpu_custom_call" | custom-call | tf_op jit(solution)/shard_map/pallas_call | solution.py:344
  100.0 1.5 slice_convert_fusion.2
  101.6 2.1 %multiply_convert_fusion.6 = (bf16[512,512]{1,0:T(8,128)(2,1)S(1)}, bf16[512,512]{1,0:T(8,128)(2,1)}) fusion(f32[528,512]{1,0:T(8,128)S(1)} %get-tuple-element.27, f32[512]{0:T(512)S(1)} %bitcast.101, f32[512]{0:T(512)S(1)} %bitcast.100, f32[512]{0:T(512)S(1)} %bitcast.99, f32[512]{0:T(512)S(1)} %bitcast.98, f32[528,512]{1,0:T(8,128)S(1)} %get-tuple-element.26, ...), kind=kLoop, calls=%fused_computation.62 | loop fusion | flops 6291456 | bytes 9453568 | tf_op jit(solution)/shard_map/convert_element_type | solution.py:421
  104.2 0.6 bitcast_exponential_fusion
  104.8 1.5 slice_convert_fusion
  106.4 1.3 multiply_convert_fusion.4
  108.5 1.5 multiply_convert_fusion.3
  110.3 2.4 %multiply_reduce_fusion.1 = (bf16[4,4,64,128]{3,2,1,0:T(8,128)(2,1)}, f32[4,4,4,64,128]{4,3,2,1,0:T(8,128)S(1)}) fusion(f32[4,4,4]{2,1,0:T(4,128)S(1)} %bitcast.86, bf16[4,128,4,128,1]{3,2,1,0,4:T(4,128)(2,1)S(1)} %bitcast.74, bf16[4,128,4,4,64]{1,0,4,3,2:T(4,128)(2,1)} %multiply_convert_fusion.3), kind=kOutput, calls=%fused_computation.22 | convolution fusion | flops 135135232 | bytes 3932416 | tf_op jit(solution)/shard_map/bsgkp,bsgn->bgkpn/dot_general | solution.py:454
  112.7 0.8 slice.171
  113.5 0.7 broadcast_in_dim.11.fade_ref
  114.2 16.5 %shard_map.128 = bf16[8,2,64,128]{3,2,1,0:T(8,128)(2,1)} custom-call(bf16[8,2,64,128]{3,2,1,0:T(8,128)(2,1)} %bitcast.78, f32[8,2,1,128]{3,2,1,0:T(1,128)} %broadcast_in_dim.11.fade_ref), custom_call_target="tpu_custom_call" | custom-call | tf_op jit(solution)/shard_map/pallas_call | solution.py:312
  131.2 2.0 %fusion.55 = (bf16[1,4,4,64,128]{4,3,2,1,0:T(8,128)(2,1)S(1)}, bf16[1,4,4,64,128]{4,3,2,1,0:T(8,128)(2,1)}, bf16[1,4,4,64,128]{4,3,2,1,0:T(8,128)(2,1)}) fusion(f32[4,4,4,64,128]{4,3,2,1,0:T(8,128)S(1)} %get-tuple-element.48, f32[4,4]{1,0:T(4,128)S(1)} %exp.91, f32[4,4]{1,0:T(4,128)S(1)} %exp.89, bf16[1,4,4,64,128]{4,3,2,1,0:T(8,128)(2,1)} %bitcast.76, ...), kind=kLoop, calls=%fused_computation.109 | loop fusion | flops 1310720 | bytes 2621632 | tf_op jit(solution)/shard_map/convert.4
  133.2 1.3 reshape.139
  135.1 1.5 %fusion.1 = f32[4,4,4,64,128]{4,3,2,1,0:T(8,128)S(1)} fusion(f32[4,4,4,128]{3,2,1,0:T(4,128)S(1)} %copy.41, f32[4,4,4,128]{3,2,1,0:T(4,128)S(1)} %bitcast.82, f32[4,4,128,128]{3,2,1,0:T(8,128)S(1)} %fusion.41, pred[128,128]{1,0:T(8,128)(4,1)S(1)} %iota_compare_fusion, bf16[4,128,4,4,64]{1,0,4,3,2:T(4,128)(2,1)S(1)} %copy-done.2), kind=kOutput, calls=%fused_computation.5 | convolution fusion | flops 140509184 | bytes 4276224 | tf_op jit(solution)/shard_map/bgkts,bsgkp->btgkp/dot_general | solution.py:448
  137.1 3.3 %copy.59 = f32[4,128,4,4,64]{4,3,2,1,0:T(4,128)} copy(f32[4,128,4,4,64]{1,4,3,2,0:T(8,128)S(1)} %fusion.17) | data formatting | bytes 4194304 | tf_op jit(solution)/shard_map/convert_element_type | solution.py:528
  140.5 4.5 %reshape.147 = f32[512,1024]{1,0:T(8,128)S(1)} reshape(f32[4,128,4,4,64]{4,3,2,1,0:T(4,128)} %copy.59) | data formatting | bytes 4194304 | tf_op jit(solution)/shard_map/convert_element_type | solution.py:528
  145.0 1.9 %multiply_reduce_fusion = f32[512]{0:T(512)S(1)} fusion(f32[512,1024]{1,0:T(8,128)S(1)} %reshape.147, bf16[528,3072]{1,0:T(8,128)(2,1)} %get-tuple-element.20), kind=kLoop, calls=%fused_computation.21 | loop fusion | flops 4193792 | bytes 3147776 | tf_op jit(solution)/shard_map/reduce_sum | solution.py:529
  147.0 6.6 %fusion = bf16[1,512,2048]{2,1,0:T(8,128)(2,1)} fusion(bf16[2048,1024]{1,0:T(8,128)(2,1)} %bitcast.102, f32[1024]{0:T(1024)S(1)} %copy-done.16, f32[512]{0:T(512)S(1)} %add_rsqrt_fusion, f32[512,1024]{1,0:T(8,128)S(1)} %reshape.147, bf16[528,3072]{1,0:T(8,128)(2,1)} %get-tuple-element.20), kind=kOutput, calls=%fused_computation.2 | convolution fusion | flops 2153250816 | bytes 9443328 | tf_op jit(solution)/shard_map/dot_general | solution.py:531
  (66 shorter events, 3.4 us)
Async XLA Ops:
  0.0 0.8 copy-start
  0.0 5.1 %copy-start.8 = (bf16[64,1024]{1,0:T(8,128)(2,1)S(1)}, bf16[64,1024]{1,0:T(8,128)(2,1)}, u32[]{:S(2)}) copy-start(bf16[64,1024]{1,0:T(8,128)(2,1)} %param.16) | copy-start | bytes 393220
  0.0 5.1 %copy-start.11 = (bf16[64,512]{1,0:T(8,128)(2,1)S(1)}, bf16[64,512]{1,0:T(8,128)(2,1)}, u32[]{:S(2)}) copy-start(bf16[64,512]{1,0:T(8,128)(2,1)} %param.18) | copy-start | bytes 196612
  0.0 5.2 %copy-start.12 = (bf16[64,512]{1,0:T(8,128)(2,1)S(1)}, bf16[64,512]{1,0:T(8,128)(2,1)}, u32[]{:S(2)}) copy-start(bf16[64,512]{1,0:T(8,128)(2,1)} %param.19) | copy-start | bytes 196612
  0.0 5.2 %copy-start.9 = (bf16[64,1024]{1,0:T(8,128)(2,1)S(1)}, bf16[64,1024]{1,0:T(8,128)(2,1)}, u32[]{:S(2)}) copy-start(bf16[64,1024]{1,0:T(8,128)(2,1)} %param.17) | copy-start | bytes 393220
  0.0 5.2 %copy-start.10 = (bf16[1024,64]{0,1:T(8,128)(2,1)S(1)}, bf16[1024,64]{0,1:T(8,128)(2,1)}, u32[]{:S(2)}) copy-start(bf16[1024,64]{0,1:T(8,128)(2,1)} %param.27) | copy-start | bytes 393220
  5.2 1.6 %copy-start.6 = (bf16[64,4096]{1,0:T(8,128)(2,1)}, bf16[64,4096]{1,0:T(8,128)(2,1)S(1)}, u32[]{:S(2)}) copy-start(bf16[64,4096]{1,0:T(8,128)(2,1)S(1)} %bitcast_dynamic-update-slice_fusion) | copy-start | bytes 1572868
  100.0 1.5 %copy-start.14 = (bf16[4,512]{1,0:T(4,128)(2,1)S(1)}, bf16[4,512]{1,0:T(4,128)(2,1)}, u32[]{:S(2)}) copy-start(bf16[4,512]{1,0:T(4,128)(2,1)} %param.23) | copy-start | bytes 12292
  100.0 1.6 %copy-start.15 = (bf16[4,512]{1,0:T(4,128)(2,1)S(1)}, bf16[4,512]{1,0:T(4,128)(2,1)}, u32[]{:S(2)}) copy-start(bf16[4,512]{1,0:T(4,128)(2,1)} %param.22) | copy-start | bytes 12292
  103.7 2.7 %copy-start.13 = (bf16[4,1024]{1,0:T(4,128)(2,1)S(1)}, bf16[4,1024]{1,0:T(4,128)(2,1)}, u32[]{:S(2)}) copy-start(bf16[4,1024]{1,0:T(4,128)(2,1)} %param.21) | copy-start | bytes 24580
  108.5 1.7 %copy-start.1 = (bf16[4,128,4,4,64]{1,0,4,3,2:T(4,128)(2,1)}, bf16[4,128,4,4,64]{1,0,4,3,2:T(4,128)(2,1)S(1)}, u32[]{:S(2)}) copy-start(bf16[4,128,4,4,64]{1,0,4,3,2:T(4,128)(2,1)S(1)} %reshape.138) | copy-start | bytes 3145732
  133.2 1.8 %copy-start.2 = (bf16[4,128,4,4,64]{1,0,4,3,2:T(4,128)(2,1)S(1)}, bf16[4,128,4,4,64]{1,0,4,3,2:T(4,128)(2,1)}, u32[]{:S(2)}) copy-start(bf16[4,128,4,4,64]{1,0,4,3,2:T(4,128)(2,1)} %copy-done.1) | copy-start | bytes 3145732
  135.0 1.6 %copy-start.3 = (bf16[8,2,64,128]{3,2,1,0:T(8,128)(2,1)S(1)}, bf16[8,2,64,128]{3,2,1,0:T(8,128)(2,1)}, u32[]{:S(2)}) copy-start(bf16[8,2,64,128]{3,2,1,0:T(8,128)(2,1)} %shard_map.128) | copy-start | bytes 786436
  135.0 1.6 %copy-start.4 = (bf16[1,4,4,64,128]{4,3,2,1,0:T(8,128)(2,1)S(1)}, bf16[1,4,4,64,128]{4,3,2,1,0:T(8,128)(2,1)}, u32[]{:S(2)}) copy-start(bf16[1,4,4,64,128]{4,3,2,1,0:T(8,128)(2,1)} %get-tuple-element.29) | copy-start | bytes 786436
  135.0 1.6 %copy-start.5 = (bf16[1,4,4,64,128]{4,3,2,1,0:T(8,128)(2,1)S(1)}, bf16[1,4,4,64,128]{4,3,2,1,0:T(8,128)(2,1)}, u32[]{:S(2)}) copy-start(bf16[1,4,4,64,128]{4,3,2,1,0:T(8,128)(2,1)} %get-tuple-element.30) | copy-start | bytes 786436
  135.0 1.6 %copy-start.7 = (f32[4,128,16]{1,2,0:T(8,128)S(1)}, f32[4,128,16]{1,2,0:T(8,128)}, u32[]{:S(2)}) copy-start(f32[4,128,16]{1,2,0:T(8,128)} %get-tuple-element.31) | copy-start | bytes 98308
  145.0 2.0 %copy-start.16 = (f32[1024]{0:T(1024)S(1)}, f32[1024]{0:T(1024)}, u32[]{:S(2)}) copy-start(f32[1024]{0:T(1024)} %param.26) | copy-start | bytes 12292
